TPU v7x, 32 devices: a whole 2x2x4 slice. The times are simulated.
32 devices in a mesh: grp: 2 (over x), ep: 16 (over z, y, core).
Axes of the slice: x: 2, y: 2, z: 4, core: 2. Of those that a mesh axis runs over, the one named last changes fastest.
Arguments:
- tokens: bfloat16 [1024, 2048], P(('grp', 'ep')), parts along dimension 0, may hold values from -6 to 6
- routing: int32 [1024, 4], P(('grp', 'ep')), parts along dimension 0, may hold values from 0 to 15, as said below
- gate_weights: float32 [1024, 4], P(('grp', 'ep')), parts along dimension 0, may hold values from 0.05 to 1
- pre_gain: float32 [2048], replicated, may hold values from 0.1 to 1.9
- w_gate: bfloat16 [16, 2048, 512], P('ep'), may hold values from -0.125 to 0.125
- w_up: bfloat16 [16, 2048, 512], P('ep'), may hold values from -0.125 to 0.125
- w_down: bfloat16 [16, 512, 2048], P('ep'), may hold values from -0.25 to 0.25
- post_gain: float32 [2048], replicated, may hold values from 0.1 to 1.9
Outputs:
- mixed_out: bfloat16 [1024, 2048], P(('grp', 'ep')), parts along dimension 0
There are 2 independent parts, one for each index of `grp`. A program takes and returns all parts, laid end to end along the dimension named above; an argument that names none is the same for every part. Nothing has to cross between parts.
Inputs may be any that keep to these rules, and one draw needn't show every extreme that they name: `routing`: each row names 4 different experts of one group (experts g * 8 to g * 8 + 7). The rows of one device name any one expert at most 16 times, and some expert exactly 16 times.
All inputs are finite; a program needn't handle non-finite values.
Results may differ from a plain program's by a relative error of at most 0.0085.
Values may be sent and summed in bfloat16 or wider, within the bound.
No kernel may reach another device: no remote copies, remote signals or barrier semaphores. Data moves between devices by JAX's collectives and lax.ppermute only.
A program may use at most 64 MiB of HBM per device.

v0:
```python
import jax
import jax.numpy as jnp
from jax import lax
from jax.experimental import pallas as pl
from jax.experimental.pallas import tpu as pltpu
from jax.sharding import PartitionSpec as P

epsilon = 1e-06
QUAD = 4
PARTS = 3


def pack_kernel(
    tokens_hbm, routing_hbm, weights_hbm, gain_hbm, out_ref, tokens_ref, routing_ref, weights_ref,
    gain_ref, sems, *, experts, extra
):
    copies = [
        pltpu.make_async_copy(source, target, sems.at[i])
        for i, (source, target) in enumerate(
            [
                (tokens_hbm, tokens_ref),
                (routing_hbm, routing_ref),
                (weights_hbm, weights_ref),
                (gain_hbm, gain_ref),
            ]
        )
    ]
    for copy in copies:
        copy.start()
    for copy in copies:
        copy.wait()
    rows, width = tokens_ref.shape
    floats = tokens_ref[...].astype(jnp.float32)
    scale = lax.rsqrt(jnp.mean(floats * floats, axis=-1, keepdims=True) + epsilon)
    out_ref[:, :width] = (floats * scale * gain_ref[...]).astype(jnp.bfloat16)
    expert = lax.broadcasted_iota(jnp.int32, (experts, rows), 0)
    dense = jnp.zeros((experts, rows), jnp.float32)
    for k in range(routing_ref.shape[0]):
        dense = dense + jnp.where(
            routing_ref[k : k + 1, :] == expert, weights_ref[k : k + 1, :], 0.0
        )
    pieces = []
    for _ in range(PARTS):
        piece = dense.astype(jnp.bfloat16)
        pieces.append(piece)
        dense = dense - piece.astype(jnp.float32)
    if extra > PARTS * experts:
        pieces.append(jnp.zeros((extra - PARTS * experts, rows), jnp.bfloat16))
    table = jnp.concatenate(pieces, axis=0)
    eye = (
        lax.broadcasted_iota(jnp.int32, (rows, rows), 0)
        == lax.broadcasted_iota(jnp.int32, (rows, rows), 1)
    ).astype(jnp.bfloat16)
    flipped = lax.dot_general(
        eye, table, (((1,), (1,)), ((), ())), preferred_element_type=jnp.float32
    )
    out_ref[:, width:] = flipped.astype(jnp.bfloat16)


def load_kernel(*refs):
    sems = refs[-1]
    count = len(refs) // 2
    copies = [
        pltpu.make_async_copy(refs[i], refs[count + i], sems.at[i]) for i in range(count)
    ]
    for copy in copies:
        copy.start()
    for copy in copies:
        copy.wait()


def expert_kernel(
    me_ref, mine_ref, other_ref, gate_ref, up_ref, down_ref, keep_ref, send_ref, *, experts
):
    rows, _ = mine_ref.shape
    width = gate_ref.shape[1]
    both = jnp.concatenate([mine_ref[...], other_ref[...]], axis=0)
    values = both[:, :width]
    table = both[:, width:].astype(jnp.float32)
    lane = lax.broadcasted_iota(jnp.int32, table.shape, 1)
    chosen = (lane % experts == me_ref[0]) & (lane < PARTS * experts)
    weight = jnp.sum(jnp.where(chosen, table, 0.0), axis=1, keepdims=True)
    gate = jnp.dot(values, gate_ref[0], preferred_element_type=jnp.float32)
    upward = jnp.dot(values, up_ref[0], preferred_element_type=jnp.float32)
    hidden = (gate / (1.0 + jnp.exp(-gate)) * upward).astype(jnp.bfloat16)
    served = jnp.dot(hidden, down_ref[0], preferred_element_type=jnp.float32) * weight
    keep_ref[...] = served[:rows]
    send_ref[...] = served[rows:].astype(jnp.bfloat16)


def finish_kernel(*refs):
    *parts, gain_ref, out_ref = refs
    mixture = parts[0][...].astype(jnp.float32)
    for part in parts[1:]:
        mixture = mixture + part[...].astype(jnp.float32)
    scale = lax.rsqrt(jnp.mean(mixture * mixture, axis=-1, keepdims=True) + epsilon)
    out_ref[...] = (mixture * scale * gain_ref[...]).astype(jnp.bfloat16)


IN_HBM = pl.BlockSpec(memory_space=pltpu.HBM)
IN_VMEM = pl.BlockSpec(memory_space=pltpu.VMEM)
IN_SMEM = pl.BlockSpec(memory_space=pltpu.SMEM)


def low(j):
    return j & -j


def body(tokens, routing, gate_weights, pre_gain, w_gate, w_up, w_down, post_gain):
    rows, width = tokens.shape
    choices = routing.shape[1]
    devices = lax.axis_size("ep")
    extra = -(-PARTS * devices // 128) * 128
    slabs = devices // QUAD
    me = lax.axis_index("ep").astype(jnp.int32).reshape(1)

    def swap(values, bits):
        return lax.ppermute(values, "ep", [(i, i ^ bits) for i in range(devices)])

    packed = pl.pallas_call(
        lambda *refs: pack_kernel(*refs, experts=devices, extra=extra),
        out_shape=jax.ShapeDtypeStruct((rows, width + extra), jnp.bfloat16),
        in_specs=[IN_HBM] * 4,
        out_specs=IN_VMEM,
        scratch_shapes=[
            pltpu.VMEM((rows, width), tokens.dtype),
            pltpu.VMEM((choices, rows), routing.dtype),
            pltpu.VMEM((choices, rows), gate_weights.dtype),
            pltpu.VMEM((1, width), pre_gain.dtype),
            pltpu.SemaphoreType.DMA((4,)),
        ],
        name="pack_kernel",
        compiler_params=pltpu.CompilerParams(vmem_limit_bytes=4 << 20),
    )(tokens, routing.T, gate_weights.T, pre_gain.reshape(1, width))

    blocks = {0: packed}
    for j in range(1, slabs):
        blocks[j] = swap(blocks[j ^ low(j)], QUAD * low(j))

    weights = pl.pallas_call(
        load_kernel,
        out_shape=[jax.ShapeDtypeStruct(w.shape, w.dtype) for w in (w_gate, w_up, w_down)],
        in_specs=[IN_HBM] * 3,
        out_specs=[IN_VMEM] * 3,
        scratch_shapes=[pltpu.SemaphoreType.DMA((3,))],
        name="load_kernel",
        compiler_params=pltpu.CompilerParams(vmem_limit_bytes=16 << 20),
    )(w_gate, w_up, w_down)

    serve = pl.pallas_call(
        lambda *refs: expert_kernel(*refs, experts=devices),
        out_shape=(
            jax.ShapeDtypeStruct((2 * rows, width), jnp.float32),
            jax.ShapeDtypeStruct((2 * rows, width), jnp.bfloat16),
        ),
        in_specs=[IN_SMEM] + [IN_VMEM] * 5,
        name="expert_kernel",
        compiler_params=pltpu.CompilerParams(vmem_limit_bytes=16 << 20),
    )
    home = {}
    for j in range(slabs):
        column = jnp.concatenate([blocks[j], swap(blocks[j], 2)], axis=0)
        other = swap(column, 1)
        keep, send = serve(me, column, other, *weights)
        column = keep + swap(send, 1).astype(jnp.float32)
        back = swap(column[rows:].astype(jnp.bfloat16), 2)
        total = column[:rows] + back.astype(jnp.float32)
        home[j] = total if j == 0 else swap(total.astype(jnp.bfloat16), QUAD * j)
    return pl.pallas_call(
        finish_kernel,
        out_shape=jax.ShapeDtypeStruct((rows, width), jnp.bfloat16),
        name="finish_kernel",
        compiler_params=pltpu.CompilerParams(vmem_limit_bytes=4 << 20),
    )(*[home[j] for j in range(slabs)], post_gain.reshape(1, width))


def solution(mesh):
    in_specs = (
        P(("grp", "ep"), None),
        P(("grp", "ep"), None),
        P(("grp", "ep"), None),
        P(),
        P("ep", None, None),
        P("ep", None, None),
        P("ep", None, None),
        P(),
    )
    out_specs = P(("grp", "ep"), None)

    return jax.shard_map(body, mesh=mesh, in_specs=in_specs, out_specs=out_specs, check_vma=False)
```

profile of v0, /device:TPU:0, one launch (start us, length us, event | category | flops | bytes accessed | tf_op | source)
XLA Modules:
  0.0 59.2 jit_solution(10580995043058482427)
XLA Ops:
  0.0 0.0 copy-start.3
  0.0 0.9 %copy-done.3 = bf16[32,2048]{1,0:T(8,128)(2,1)S(1)} copy-done((bf16[32,2048]{1,0:T(8,128)(2,1)S(1)}, bf16[32,2048]{1,0:T(8,128)(2,1)}, u32[]{:S(2)}) %copy-start.3) | copy-done | bytes 131096
  0.9 0.7 %copy-done.5 = f32[2048]{0:T(1024)S(1)} copy-done((f32[2048]{0:T(1024)S(1)}, f32[2048]{0:T(1024)}, u32[]{:S(2)}) %copy-start.5) | copy-done | bytes 8216
  1.6 0.7 %copy-done.6 = s32[32,4]{0,1:T(4,128)S(1)} copy-done((s32[32,4]{0,1:T(4,128)S(1)}, s32[32,4]{0,1:T(4,128)}, u32[]{:S(2)}) %copy-start.6) | copy-done | bytes 536
  2.3 0.7 %copy-done.7 = f32[32,4]{0,1:T(4,128)S(1)} copy-done((f32[32,4]{0,1:T(4,128)S(1)}, f32[32,4]{0,1:T(4,128)}, u32[]{:S(2)}) %copy-start.7) | copy-done | bytes 536
  3.0 0.3 pack_kernel.1
  3.3 3.1 %collective-permute-start = (bf16[32,2176]{1,0:T(8,128)(2,1)S(1)}, bf16[32,2176]{1,0:T(8,128)(2,1)S(1)}, u32[]{:S(2)}, u32[]{:S(2)}) collective-permute-start(bf16[32,2176]{1,0:T(8,128)(2,1)S(1)} %pack_kernel.1), channel_id=1, source_target_pairs={{0,2},{1,3},{2,0},{3,1},{4,6},{5,7},{6,4},{7,5},{8,10},{9,11},{10,... | collective-permute-start | bytes 417800 | tf_op jit(solution)/shard_map/ppermute | solution.py:118
  6.4 2.6 %collective-permute-start.10 = (bf16[32,2176]{1,0:T(8,128)(2,1)S(1)}, bf16[32,2176]{1,0:T(8,128)(2,1)S(1)}, u32[]{:S(2)}, u32[]{:S(2)}) collective-permute-start(bf16[32,2176]{1,0:T(8,128)(2,1)S(1)} %pack_kernel.1), channel_id=1, source_target_pairs={{0,8},{1,9},{2,10},{3,11},{4,12},{5,13},{6,14},{7,15},{8,0},{9,1},... | collective-permute-start | bytes 417800 | tf_op jit(solution)/shard_map/ppermute | solution.py:118
  9.0 1.6 %collective-permute-start.4 = (bf16[32,2176]{1,0:T(8,128)(2,1)S(1)}, bf16[32,2176]{1,0:T(8,128)(2,1)S(1)}, u32[]{:S(2)}, u32[]{:S(2)}) collective-permute-start(bf16[32,2176]{1,0:T(8,128)(2,1)S(1)} %pack_kernel.1), channel_id=1, source_target_pairs={{0,4},{1,5},{2,6},{3,7},{4,0},{5,1},{6,2},{7,3},{8,12},{9,13},{10,... | collective-permute-start | bytes 417800 | tf_op jit(solution)/shard_map/ppermute | solution.py:118
  10.5 1.6 %copy-done = bf16[1,2048,512]{2,1,0:T(8,128)(2,1)S(1)} copy-done((bf16[1,2048,512]{2,1,0:T(8,128)(2,1)S(1)}, bf16[1,2048,512]{2,1,0:T(8,128)(2,1)}, u32[]{:S(2)}) %copy-start) | copy-done | bytes 2097176
  12.1 1.6 %copy-done.1 = bf16[1,2048,512]{2,1,0:T(8,128)(2,1)S(1)} copy-done((bf16[1,2048,512]{2,1,0:T(8,128)(2,1)S(1)}, bf16[1,2048,512]{2,1,0:T(8,128)(2,1)}, u32[]{:S(2)}) %copy-start.1) | copy-done | bytes 2097176
  13.7 1.6 %copy-done.2 = bf16[1,512,2048]{2,1,0:T(8,128)(2,1)S(1)} copy-done((bf16[1,512,2048]{2,1,0:T(8,128)(2,1)S(1)}, bf16[1,512,2048]{2,1,0:T(8,128)(2,1)}, u32[]{:S(2)}) %copy-start.2) | copy-done | bytes 2097176
  15.3 0.5 load_kernel.1
  15.8 0.0 collective-permute-done
  15.8 0.1 collective-permute-start.1
  15.9 0.0 collective-permute-done.10
  15.9 0.5 collective-permute-start.16
  16.4 0.6 collective-permute-start.11
  17.0 0.0 collective-permute-done.4
  17.0 1.6 %collective-permute-start.5 = (bf16[32,2176]{1,0:T(8,128)(2,1)S(1)}, bf16[32,2176]{1,0:T(8,128)(2,1)S(1)}, u32[]{:S(2)}, u32[]{:S(2)}) collective-permute-start(bf16[32,2176]{1,0:T(8,128)(2,1)S(1)} %collective-permute-done.4), channel_id=1, source_target_pairs={{0,2},{1,3},{2,0},{3,1},{4,6},{5,7},{6,4},{7,5},{8,10},{9,11},{10,... | collective-permute-start | bytes 417800 | tf_op jit(solution)/shard_map/ppermute | solution.py:118
  18.6 4.4 %collective-permute-done.11 = bf16[32,2176]{1,0:T(8,128)(2,1)S(1)} collective-permute-done((bf16[32,2176]{1,0:T(8,128)(2,1)S(1)}, bf16[32,2176]{1,0:T(8,128)(2,1)S(1)}, u32[]{:S(2)}, u32[]{:S(2)}) %collective-permute-start.11) | collective-permute-done | bytes 139296 | tf_op jit(solution)/shard_map/ppermute | solution.py:118
  23.0 0.1 collective-permute-start.12
  23.1 2.1 %collective-permute-done.5 = bf16[32,2176]{1,0:T(8,128)(2,1)S(1)} collective-permute-done((bf16[32,2176]{1,0:T(8,128)(2,1)S(1)}, bf16[32,2176]{1,0:T(8,128)(2,1)S(1)}, u32[]{:S(2)}, u32[]{:S(2)}) %collective-permute-start.5) | collective-permute-done | bytes 139296 | tf_op jit(solution)/shard_map/ppermute | solution.py:118
  25.2 0.1 collective-permute-start.6
  25.3 0.0 collective-permute-done.16
  25.3 0.6 collective-permute-start.17
  25.9 0.0 collective-permute-done.1.refs_2_
  25.9 1.1 %expert_kernel.4 = (f32[64,2048]{1,0:T(8,128)S(1)}, bf16[64,2048]{1,0:T(8,128)(2,1)S(1)}) custom-call(s32[1]{0:T(128)} %bitcast.refs_0_, bf16[64,2176]{1,0:T(8,128)(2,1)S(1)} %pad_maximum_fusion.refs_1_, bf16[64,2176]{1,0:T(8,128)(2,1)S(1)} %collective-permute-done.1.refs_2_, bf16[1,2048,512]{2,1,0:T(8,128)(2,1)S(1)} %get-tuple-element.16.refs_3_, ...), custom_call_target="tpu_custom_call" | custom-call | tf_op jit(solution)/shard_map/expert_kernel/pallas_call | solution.py:164
  27.0 0.2 collective-permute-start.2
  27.2 4.1 %collective-permute-done.17 = bf16[32,2176]{1,0:T(8,128)(2,1)S(1)} collective-permute-done((bf16[32,2176]{1,0:T(8,128)(2,1)S(1)}, bf16[32,2176]{1,0:T(8,128)(2,1)S(1)}, u32[]{:S(2)}, u32[]{:S(2)}) %collective-permute-start.17) | collective-permute-done | bytes 139296 | tf_op jit(solution)/shard_map/ppermute | solution.py:118
  31.4 0.1 collective-permute-start.18
  31.5 0.0 collective-permute-done.12.refs_2_
  31.5 1.1 %expert_kernel.6 = (f32[64,2048]{1,0:T(8,128)S(1)}, bf16[64,2048]{1,0:T(8,128)(2,1)S(1)}) custom-call(s32[1]{0:T(128)} %bitcast.refs_0_, bf16[64,2176]{1,0:T(8,128)(2,1)S(1)} %constant_dynamic-update-slice_fusion.2.refs_1_, bf16[64,2176]{1,0:T(8,128)(2,1)S(1)} %collective-permute-done.12.refs_2_, bf16[1,2048,512]{2,1,0:T(8,128)(2,1)S(1)} %get-tuple-element.16.refs_3_, ...), custom_call_target="tpu_custom_call" | custom-call | tf_op jit(solution)/shard_map/expert_kernel/pallas_call | solution.py:164
  32.6 0.5 collective-permute-start.13
  33.1 0.0 collective-permute-done.6.refs_2_
  33.1 1.1 %expert_kernel.5 = (f32[64,2048]{1,0:T(8,128)S(1)}, bf16[64,2048]{1,0:T(8,128)(2,1)S(1)}) custom-call(s32[1]{0:T(128)} %bitcast.refs_0_, bf16[64,2176]{1,0:T(8,128)(2,1)S(1)} %constant_dynamic-update-slice_fusion.refs_1_, bf16[64,2176]{1,0:T(8,128)(2,1)S(1)} %collective-permute-done.6.refs_2_, bf16[1,2048,512]{2,1,0:T(8,128)(2,1)S(1)} %get-tuple-element.16.refs_3_, ...), custom_call_target="tpu_custom_call" | custom-call | tf_op jit(solution)/shard_map/expert_kernel/pallas_call | solution.py:164
  34.3 0.1 collective-permute-start.7
  34.4 0.0 collective-permute-done.2
  34.4 0.1 convert_add_fusion.3
  34.4 0.6 collective-permute-start.3
  35.0 0.0 collective-permute-done.18.refs_2_
  35.0 1.1 %expert_kernel.7 = (f32[64,2048]{1,0:T(8,128)S(1)}, bf16[64,2048]{1,0:T(8,128)(2,1)S(1)}) custom-call(s32[1]{0:T(128)} %bitcast.refs_0_, bf16[64,2176]{1,0:T(8,128)(2,1)S(1)} %constant_dynamic-update-slice_fusion.4.refs_1_, bf16[64,2176]{1,0:T(8,128)(2,1)S(1)} %collective-permute-done.18.refs_2_, bf16[1,2048,512]{2,1,0:T(8,128)(2,1)S(1)} %get-tuple-element.16.refs_3_, ...), custom_call_target="tpu_custom_call" | custom-call | tf_op jit(solution)/shard_map/expert_kernel/pallas_call | solution.py:164
  36.1 0.3 collective-permute-start.19
  36.4 0.0 collective-permute-done.13
  36.5 1.6 %collective-permute-start.14 = (bf16[32,2048]{1,0:T(8,128)(2,1)S(1)}, bf16[32,2048]{1,0:T(8,128)(2,1)S(1)}, u32[]{:S(2)}, u32[]{:S(2)}) collective-permute-start(bf16[32,2048]{1,0:T(8,128)(2,1)S(1)} %slice.59), channel_id=1, source_target_pairs={{0,2},{1,3},{2,0},{3,1},{4,6},{5,7},{6,4},{7,5},{8,10},{9,11},{10,... | collective-permute-start | bytes 393224 | tf_op jit(solution)/shard_map/ppermute | solution.py:118
  38.1 0.0 collective-permute-done.7
  38.1 0.1 convert_add_fusion.2
  38.1 0.0 copy-start.4
  38.2 0.6 collective-permute-start.8
  38.7 5.0 %collective-permute-done.14 = bf16[32,2048]{1,0:T(8,128)(2,1)S(1)} collective-permute-done((bf16[32,2048]{1,0:T(8,128)(2,1)S(1)}, bf16[32,2048]{1,0:T(8,128)(2,1)S(1)}, u32[]{:S(2)}, u32[]{:S(2)}) %collective-permute-start.14) | collective-permute-done | bytes 131104 | tf_op jit(solution)/shard_map/ppermute | solution.py:118
  43.7 2.7 %collective-permute-start.15 = (bf16[32,2048]{1,0:T(8,128)(2,1)S(1)}, bf16[32,2048]{1,0:T(8,128)(2,1)S(1)}, u32[]{:S(2)}, u32[]{:S(2)}) collective-permute-start(bf16[32,2048]{1,0:T(8,128)(2,1)S(1)} %fusion.1), channel_id=1, source_target_pairs={{0,8},{1,9},{2,10},{3,11},{4,12},{5,13},{6,14},{7,15},{8,0},{9,1},... | collective-permute-start | bytes 393224 | tf_op jit(solution)/shard_map/ppermute | solution.py:118
  46.4 0.0 collective-permute-done.19
  46.4 0.1 convert_add_fusion
  46.5 0.8 %collective-permute-start.20 = (bf16[32,2048]{1,0:T(8,128)(2,1)S(1)}, bf16[32,2048]{1,0:T(8,128)(2,1)S(1)}, u32[]{:S(2)}, u32[]{:S(2)}) collective-permute-start(bf16[32,2048]{1,0:T(8,128)(2,1)S(1)} %slice.58), channel_id=1, source_target_pairs={{0,2},{1,3},{2,0},{3,1},{4,6},{5,7},{6,4},{7,5},{8,10},{9,11},{10,... | collective-permute-start | bytes 393224 | tf_op jit(solution)/shard_map/ppermute | solution.py:118
  47.3 0.0 collective-permute-done.8
  47.3 0.4 collective-permute-start.9
  47.7 3.8 %collective-permute-done.20 = bf16[32,2048]{1,0:T(8,128)(2,1)S(1)} collective-permute-done((bf16[32,2048]{1,0:T(8,128)(2,1)S(1)}, bf16[32,2048]{1,0:T(8,128)(2,1)S(1)}, u32[]{:S(2)}, u32[]{:S(2)}) %collective-permute-start.20) | collective-permute-done | bytes 131104 | tf_op jit(solution)/shard_map/ppermute | solution.py:118
  51.6 1.4 %collective-permute-start.21 = (bf16[32,2048]{1,0:T(8,128)(2,1)S(1)}, bf16[32,2048]{1,0:T(8,128)(2,1)S(1)}, u32[]{:S(2)}, u32[]{:S(2)}) collective-permute-start(bf16[32,2048]{1,0:T(8,128)(2,1)S(1)} %fusion), channel_id=1, source_target_pairs={{0,12},{1,13},{2,14},{3,15},{4,8},{5,9},{6,10},{7,11},{8,4},{9,5},... | collective-permute-start | bytes 393224 | tf_op jit(solution)/shard_map/ppermute | solution.py:118
  53.0 0.0 collective-permute-done.3
  53.0 0.0 collective-permute-done.15.refs_2_
  53.0 0.4 collective-permute-done.9.refs_1_
  53.4 5.0 %collective-permute-done.21.refs_3_ = bf16[32,2048]{1,0:T(8,128)(2,1)S(1)} collective-permute-done((bf16[32,2048]{1,0:T(8,128)(2,1)S(1)}, bf16[32,2048]{1,0:T(8,128)(2,1)S(1)}, u32[]{:S(2)}, u32[]{:S(2)}) %collective-permute-start.21) | collective-permute-done | bytes 131104 | tf_op jit(solution)/shard_map/ppermute | solution.py:118
  58.4 0.0 copy-done.4
  58.4 0.8 %finish_kernel.1 = bf16[32,2048]{1,0:T(8,128)(2,1)} custom-call(f32[32,2048]{1,0:T(8,128)S(1)} %slice_add_fusion.3.refs_0_, bf16[32,2048]{1,0:T(8,128)(2,1)S(1)} %collective-permute-done.9.refs_1_, bf16[32,2048]{1,0:T(8,128)(2,1)S(1)} %collective-permute-done.15.refs_2_, bf16[32,2048]{1,0:T(8,128)(2,1)S(1)} %collective-permute-done.21.refs_3_, ...), custom_call_target="tpu_custom_call" | custom-call | tf_op jit(solution)/shard_map/finish_kernel/pallas_call | solution.py:169
  (22 shorter events, 0.4 us)
Async XLA Ops:
  0.0 0.9 %copy-start.3 = (bf16[32,2048]{1,0:T(8,128)(2,1)S(1)}, bf16[32,2048]{1,0:T(8,128)(2,1)}, u32[]{:S(2)}) copy-start(bf16[32,2048]{1,0:T(8,128)(2,1)} %refs_0_.2) | copy-start | bytes 393220
  0.9 0.7 %copy-start.5 = (f32[2048]{0:T(1024)S(1)}, f32[2048]{0:T(1024)}, u32[]{:S(2)}) copy-start(f32[2048]{0:T(1024)} %param.11) | copy-start | bytes 24580
  1.6 0.7 %copy-start.6 = (s32[32,4]{0,1:T(4,128)S(1)}, s32[32,4]{0,1:T(4,128)}, u32[]{:S(2)}) copy-start(s32[32,4]{0,1:T(4,128)} %param.9) | copy-start | bytes 1540
  2.3 0.7 %copy-start.7 = (f32[32,4]{0,1:T(4,128)S(1)}, f32[32,4]{0,1:T(4,128)}, u32[]{:S(2)}) copy-start(f32[32,4]{0,1:T(4,128)} %param.10) | copy-start | bytes 1540
  3.3 12.5 %collective-permute-start = (bf16[32,2176]{1,0:T(8,128)(2,1)S(1)}, bf16[32,2176]{1,0:T(8,128)(2,1)S(1)}, u32[]{:S(2)}, u32[]{:S(2)}) collective-permute-start(bf16[32,2176]{1,0:T(8,128)(2,1)S(1)} %pack_kernel.1), channel_id=1, source_target_pairs={{0,2},{1,3},{2,0},{3,1},{4,6},{5,7},{6,4},{7,5},{8,10},{9,11},{10,... | collective-permute-start | bytes 417800 | tf_op jit(solution)/shard_map/ppermute | solution.py:118
  6.4 9.5 %collective-permute-start.10 = (bf16[32,2176]{1,0:T(8,128)(2,1)S(1)}, bf16[32,2176]{1,0:T(8,128)(2,1)S(1)}, u32[]{:S(2)}, u32[]{:S(2)}) collective-permute-start(bf16[32,2176]{1,0:T(8,128)(2,1)S(1)} %pack_kernel.1), channel_id=1, source_target_pairs={{0,8},{1,9},{2,10},{3,11},{4,12},{5,13},{6,14},{7,15},{8,0},{9,1},... | collective-permute-start | bytes 417800 | tf_op jit(solution)/shard_map/ppermute | solution.py:118
  9.0 8.0 %collective-permute-start.4 = (bf16[32,2176]{1,0:T(8,128)(2,1)S(1)}, bf16[32,2176]{1,0:T(8,128)(2,1)S(1)}, u32[]{:S(2)}, u32[]{:S(2)}) collective-permute-start(bf16[32,2176]{1,0:T(8,128)(2,1)S(1)} %pack_kernel.1), channel_id=1, source_target_pairs={{0,4},{1,5},{2,6},{3,7},{4,0},{5,1},{6,2},{7,3},{8,12},{9,13},{10,... | collective-permute-start | bytes 417800 | tf_op jit(solution)/shard_map/ppermute | solution.py:118
  10.5 1.6 %copy-start = (bf16[1,2048,512]{2,1,0:T(8,128)(2,1)S(1)}, bf16[1,2048,512]{2,1,0:T(8,128)(2,1)}, u32[]{:S(2)}) copy-start(bf16[1,2048,512]{2,1,0:T(8,128)(2,1)} %refs_0_.3) | copy-start | bytes 6291460
  12.1 1.6 %copy-start.1 = (bf16[1,2048,512]{2,1,0:T(8,128)(2,1)S(1)}, bf16[1,2048,512]{2,1,0:T(8,128)(2,1)}, u32[]{:S(2)}) copy-start(bf16[1,2048,512]{2,1,0:T(8,128)(2,1)} %refs_1_.1) | copy-start | bytes 6291460
  13.7 1.6 %copy-start.2 = (bf16[1,512,2048]{2,1,0:T(8,128)(2,1)S(1)}, bf16[1,512,2048]{2,1,0:T(8,128)(2,1)}, u32[]{:S(2)}) copy-start(bf16[1,512,2048]{2,1,0:T(8,128)(2,1)} %refs_2_.1) | copy-start | bytes 6291460
  15.8 10.1 %collective-permute-start.1 = (bf16[64,2176]{1,0:T(8,128)(2,1)S(1)}, bf16[64,2176]{1,0:T(8,128)(2,1)S(1)}, u32[]{:S(2)}, u32[]{:S(2)}) collective-permute-start(bf16[64,2176]{1,0:T(8,128)(2,1)S(1)} %pad_maximum_fusion.refs_1_), channel_id=1, source_target_pairs={{0,1},{1,0},{2,3},{3,2},{4,5},{5,4},{6,7},{7,6},{8,9},{9,8},{10,11... | collective-permute-start | bytes 835592 | tf_op jit(solution)/shard_map/ppermute | solution.py:118
  15.9 9.4 %collective-permute-start.16 = (bf16[32,2176]{1,0:T(8,128)(2,1)S(1)}, bf16[32,2176]{1,0:T(8,128)(2,1)S(1)}, u32[]{:S(2)}, u32[]{:S(2)}) collective-permute-start(bf16[32,2176]{1,0:T(8,128)(2,1)S(1)} %collective-permute-done.10), channel_id=1, source_target_pairs={{0,4},{1,5},{2,6},{3,7},{4,0},{5,1},{6,2},{7,3},{8,12},{9,13},{10,... | collective-permute-start | bytes 417800 | tf_op jit(solution)/shard_map/ppermute | solution.py:118
  16.4 6.6 %collective-permute-start.11 = (bf16[32,2176]{1,0:T(8,128)(2,1)S(1)}, bf16[32,2176]{1,0:T(8,128)(2,1)S(1)}, u32[]{:S(2)}, u32[]{:S(2)}) collective-permute-start(bf16[32,2176]{1,0:T(8,128)(2,1)S(1)} %collective-permute-done.10), channel_id=1, source_target_pairs={{0,2},{1,3},{2,0},{3,1},{4,6},{5,7},{6,4},{7,5},{8,10},{9,11},{10,... | collective-permute-start | bytes 417800 | tf_op jit(solution)/shard_map/ppermute | solution.py:118
  17.0 8.2 %collective-permute-start.5 = (bf16[32,2176]{1,0:T(8,128)(2,1)S(1)}, bf16[32,2176]{1,0:T(8,128)(2,1)S(1)}, u32[]{:S(2)}, u32[]{:S(2)}) collective-permute-start(bf16[32,2176]{1,0:T(8,128)(2,1)S(1)} %collective-permute-done.4), channel_id=1, source_target_pairs={{0,2},{1,3},{2,0},{3,1},{4,6},{5,7},{6,4},{7,5},{8,10},{9,11},{10,... | collective-permute-start | bytes 417800 | tf_op jit(solution)/shard_map/ppermute | solution.py:118
  23.0 8.4 %collective-permute-start.12 = (bf16[64,2176]{1,0:T(8,128)(2,1)S(1)}, bf16[64,2176]{1,0:T(8,128)(2,1)S(1)}, u32[]{:S(2)}, u32[]{:S(2)}) collective-permute-start(bf16[64,2176]{1,0:T(8,128)(2,1)S(1)} %constant_dynamic-update-slice_fusion.2.refs_1_), channel_id=1, source_target_pairs={{0,1},{1,0},{2,3},{3,2},{4,5},{5,4},{6,7},{7,6},{8,9},{9,8},{10,11... | collective-permute-start | bytes 835592 | tf_op jit(solution)/shard_map/ppermute | solution.py:118
  25.2 7.9 %collective-permute-start.6 = (bf16[64,2176]{1,0:T(8,128)(2,1)S(1)}, bf16[64,2176]{1,0:T(8,128)(2,1)S(1)}, u32[]{:S(2)}, u32[]{:S(2)}) collective-permute-start(bf16[64,2176]{1,0:T(8,128)(2,1)S(1)} %constant_dynamic-update-slice_fusion.refs_1_), channel_id=1, source_target_pairs={{0,1},{1,0},{2,3},{3,2},{4,5},{5,4},{6,7},{7,6},{8,9},{9,8},{10,11... | collective-permute-start | bytes 835592 | tf_op jit(solution)/shard_map/ppermute | solution.py:118
  25.3 6.1 %collective-permute-start.17 = (bf16[32,2176]{1,0:T(8,128)(2,1)S(1)}, bf16[32,2176]{1,0:T(8,128)(2,1)S(1)}, u32[]{:S(2)}, u32[]{:S(2)}) collective-permute-start(bf16[32,2176]{1,0:T(8,128)(2,1)S(1)} %collective-permute-done.16), channel_id=1, source_target_pairs={{0,2},{1,3},{2,0},{3,1},{4,6},{5,7},{6,4},{7,5},{8,10},{9,11},{10,... | collective-permute-start | bytes 417800 | tf_op jit(solution)/shard_map/ppermute | solution.py:118
  27.0 7.3 %collective-permute-start.2 = (bf16[64,2048]{1,0:T(8,128)(2,1)S(1)}, bf16[64,2048]{1,0:T(8,128)(2,1)S(1)}, u32[]{:S(2)}, u32[]{:S(2)}) collective-permute-start(bf16[64,2048]{1,0:T(8,128)(2,1)S(1)} %get-tuple-element.20), channel_id=1, source_target_pairs={{0,1},{1,0},{2,3},{3,2},{4,5},{5,4},{6,7},{7,6},{8,9},{9,8},{10,11... | collective-permute-start | bytes 786440 | tf_op jit(solution)/shard_map/ppermute | solution.py:118
  31.4 3.6 %collective-permute-start.18 = (bf16[64,2176]{1,0:T(8,128)(2,1)S(1)}, bf16[64,2176]{1,0:T(8,128)(2,1)S(1)}, u32[]{:S(2)}, u32[]{:S(2)}) collective-permute-start(bf16[64,2176]{1,0:T(8,128)(2,1)S(1)} %constant_dynamic-update-slice_fusion.4.refs_1_), channel_id=1, source_target_pairs={{0,1},{1,0},{2,3},{3,2},{4,5},{5,4},{6,7},{7,6},{8,9},{9,8},{10,11... | collective-permute-start | bytes 835592 | tf_op jit(solution)/shard_map/ppermute | solution.py:118
  32.6 3.8 %collective-permute-start.13 = (bf16[64,2048]{1,0:T(8,128)(2,1)S(1)}, bf16[64,2048]{1,0:T(8,128)(2,1)S(1)}, u32[]{:S(2)}, u32[]{:S(2)}) collective-permute-start(bf16[64,2048]{1,0:T(8,128)(2,1)S(1)} %get-tuple-element.24), channel_id=1, source_target_pairs={{0,1},{1,0},{2,3},{3,2},{4,5},{5,4},{6,7},{7,6},{8,9},{9,8},{10,11... | collective-permute-start | bytes 786440 | tf_op jit(solution)/shard_map/ppermute | solution.py:118
  34.3 3.8 %collective-permute-start.7 = (bf16[64,2048]{1,0:T(8,128)(2,1)S(1)}, bf16[64,2048]{1,0:T(8,128)(2,1)S(1)}, u32[]{:S(2)}, u32[]{:S(2)}) collective-permute-start(bf16[64,2048]{1,0:T(8,128)(2,1)S(1)} %get-tuple-element.22), channel_id=1, source_target_pairs={{0,1},{1,0},{2,3},{3,2},{4,5},{5,4},{6,7},{7,6},{8,9},{9,8},{10,11... | collective-permute-start | bytes 786440 | tf_op jit(solution)/shard_map/ppermute | solution.py:118
  34.4 18.5 %collective-permute-start.3 = (bf16[32,2048]{1,0:T(8,128)(2,1)S(1)}, bf16[32,2048]{1,0:T(8,128)(2,1)S(1)}, u32[]{:S(2)}, u32[]{:S(2)}) collective-permute-start(bf16[32,2048]{1,0:T(8,128)(2,1)S(1)} %slice.61), channel_id=1, source_target_pairs={{0,2},{1,3},{2,0},{3,1},{4,6},{5,7},{6,4},{7,5},{8,10},{9,11},{10,... | collective-permute-start | bytes 393224 | tf_op jit(solution)/shard_map/ppermute | solution.py:118
  36.1 10.3 %collective-permute-start.19 = (bf16[64,2048]{1,0:T(8,128)(2,1)S(1)}, bf16[64,2048]{1,0:T(8,128)(2,1)S(1)}, u32[]{:S(2)}, u32[]{:S(2)}) collective-permute-start(bf16[64,2048]{1,0:T(8,128)(2,1)S(1)} %get-tuple-element.26), channel_id=1, source_target_pairs={{0,1},{1,0},{2,3},{3,2},{4,5},{5,4},{6,7},{7,6},{8,9},{9,8},{10,11... | collective-permute-start | bytes 786440 | tf_op jit(solution)/shard_map/ppermute | solution.py:118
  36.5 7.2 %collective-permute-start.14 = (bf16[32,2048]{1,0:T(8,128)(2,1)S(1)}, bf16[32,2048]{1,0:T(8,128)(2,1)S(1)}, u32[]{:S(2)}, u32[]{:S(2)}) collective-permute-start(bf16[32,2048]{1,0:T(8,128)(2,1)S(1)} %slice.59), channel_id=1, source_target_pairs={{0,2},{1,3},{2,0},{3,1},{4,6},{5,7},{6,4},{7,5},{8,10},{9,11},{10,... | collective-permute-start | bytes 393224 | tf_op jit(solution)/shard_map/ppermute | solution.py:118
  38.1 20.3 %copy-start.4 = (f32[2048]{0:T(1024)S(1)}, f32[2048]{0:T(1024)}, u32[]{:S(2)}) copy-start(f32[2048]{0:T(1024)} %param.15) | copy-start | bytes 24580
  38.2 9.1 %collective-permute-start.8 = (bf16[32,2048]{1,0:T(8,128)(2,1)S(1)}, bf16[32,2048]{1,0:T(8,128)(2,1)S(1)}, u32[]{:S(2)}, u32[]{:S(2)}) collective-permute-start(bf16[32,2048]{1,0:T(8,128)(2,1)S(1)} %slice.60), channel_id=1, source_target_pairs={{0,2},{1,3},{2,0},{3,1},{4,6},{5,7},{6,4},{7,5},{8,10},{9,11},{10,... | collective-permute-start | bytes 393224 | tf_op jit(solution)/shard_map/ppermute | solution.py:118
  43.7 9.3 %collective-permute-start.15 = (bf16[32,2048]{1,0:T(8,128)(2,1)S(1)}, bf16[32,2048]{1,0:T(8,128)(2,1)S(1)}, u32[]{:S(2)}, u32[]{:S(2)}) collective-permute-start(bf16[32,2048]{1,0:T(8,128)(2,1)S(1)} %fusion.1), channel_id=1, source_target_pairs={{0,8},{1,9},{2,10},{3,11},{4,12},{5,13},{6,14},{7,15},{8,0},{9,1},... | collective-permute-start | bytes 393224 | tf_op jit(solution)/shard_map/ppermute | solution.py:118
  46.5 5.0 %collective-permute-start.20 = (bf16[32,2048]{1,0:T(8,128)(2,1)S(1)}, bf16[32,2048]{1,0:T(8,128)(2,1)S(1)}, u32[]{:S(2)}, u32[]{:S(2)}) collective-permute-start(bf16[32,2048]{1,0:T(8,128)(2,1)S(1)} %slice.58), channel_id=1, source_target_pairs={{0,2},{1,3},{2,0},{3,1},{4,6},{5,7},{6,4},{7,5},{8,10},{9,11},{10,... | collective-permute-start | bytes 393224 | tf_op jit(solution)/shard_map/ppermute | solution.py:118
  47.3 6.1 %collective-permute-start.9 = (bf16[32,2048]{1,0:T(8,128)(2,1)S(1)}, bf16[32,2048]{1,0:T(8,128)(2,1)S(1)}, u32[]{:S(2)}, u32[]{:S(2)}) collective-permute-start(bf16[32,2048]{1,0:T(8,128)(2,1)S(1)} %fusion.2), channel_id=1, source_target_pairs={{0,4},{1,5},{2,6},{3,7},{4,0},{5,1},{6,2},{7,3},{8,12},{9,13},{10,... | collective-permute-start | bytes 393224 | tf_op jit(solution)/shard_map/ppermute | solution.py:118
  51.6 6.8 %collective-permute-start.21 = (bf16[32,2048]{1,0:T(8,128)(2,1)S(1)}, bf16[32,2048]{1,0:T(8,128)(2,1)S(1)}, u32[]{:S(2)}, u32[]{:S(2)}) collective-permute-start(bf16[32,2048]{1,0:T(8,128)(2,1)S(1)} %fusion), channel_id=1, source_target_pairs={{0,12},{1,13},{2,14},{3,15},{4,8},{5,9},{6,10},{7,11},{8,4},{9,5},... | collective-permute-start | bytes 393224 | tf_op jit(solution)/shard_map/ppermute | solution.py:118
where the time goes:
time: 59.5 us; the launch traced here: 59.2 us
  waiting for transfers between devices  24.9 us (42%)
  starting transfers between devices  19.8 us (33%)
  local copies, waits for them, and re-layouts  7.89 us (13%)
  Pallas kernels  6.02 us (10%)
    ppermute x22, waiting for transfers between devices, swap(): return lax.ppermute(values, 'ep', [(i, i ^ bits) for i in range(devices)])  24.9 us
    ppermute x22, starting transfers between devices, swap(): return lax.ppermute(values, 'ep', [(i, i ^ bits) for i in range(devices)])  19.8 us
    unnamed x19, local copies, waits for them, and re-layouts  7.77 us
    pallas_call x4, Pallas kernels, body(): keep, send = serve(me, column, other, *weights)  4.43 us
  transfers between devices with their start and end apart: 22, of which 7 were waited for; matrix products, arithmetic and copies ran while one was open for 1% of the time, Pallas kernels for 8%

commit v1 on v0

--- a/solution.py
+++ b/solution.py
@@ -97,6 +97,10 @@
     out_ref[...] = (mixture * scale * gain_ref[...]).astype(jnp.bfloat16)
 
 
+def in_hbm(values):
+    return pltpu.with_memory_space_constraint(values, pltpu.HBM)
+
+
 IN_HBM = pl.BlockSpec(memory_space=pltpu.HBM)
 IN_VMEM = pl.BlockSpec(memory_space=pltpu.VMEM)
 IN_SMEM = pl.BlockSpec(memory_space=pltpu.SMEM)
@@ -131,7 +135,7 @@
         ],
         name="pack_kernel",
         compiler_params=pltpu.CompilerParams(vmem_limit_bytes=4 << 20),
-    )(tokens, routing.T, gate_weights.T, pre_gain.reshape(1, width))
+    )(*map(in_hbm, (tokens, routing.T, gate_weights.T, pre_gain.reshape(1, width))))
 
     blocks = {0: packed}
     for j in range(1, slabs):
@@ -144,8 +148,8 @@
         out_specs=[IN_VMEM] * 3,
         scratch_shapes=[pltpu.SemaphoreType.DMA((3,))],
         name="load_kernel",
-        compiler_params=pltpu.CompilerParams(vmem_limit_bytes=16 << 20),
-    )(w_gate, w_up, w_down)
+        compiler_params=pltpu.CompilerParams(vmem_limit_bytes=4 << 20),
+    )(*map(in_hbm, (w_gate, w_up, w_down)))
 
     serve = pl.pallas_call(
         lambda *refs: expert_kernel(*refs, experts=devices),

time: 59.5 us -> 57.2 us (0.961)
  local copies, waits for them, and re-layouts: 7.89 us -> 0.15 us
  Pallas kernels: 6.02 us -> 9.22 us
  waiting for transfers between devices: 24.9 us -> 27.7 us
    unnamed x19 -> x5, local copies, waits for them, and re-layouts: 7.77 us -> 0.04 us
    ppermute x22, waiting for transfers between devices: 24.9 us -> 27.7 us  [swap(): return lax.ppermute(values, 'ep', [(i, i ^ bits) for i in range(devices)])]
    pallas_call x1, Pallas kernels: 0.45 us -> 2.88 us  [body(): pl.pallas_call(load_kernel, out_shape=[jax.ShapeDtypeStruct(w.shape, w.dt...]
    pallas_call x1, Pallas kernels: 0.33 us -> 1.08 us  [body(): pl.pallas_call(lambda *refs: pack_kernel(*refs, experts=devices, extra=ex...]
  transfers between devices with their start and end apart: 22 -> 22, of which waited for: 7 -> 9; matrix products, arithmetic and copies ran while one was open for 1% -> 1% of each run, Pallas kernels for 8% -> 13%
where the time goes in v1:
time: 57.2 us; the launch traced here: 57 us
  waiting for transfers between devices  27.7 us (48%)
  starting transfers between devices  19.4 us (34%)
  Pallas kernels  9.22 us (16%)
    ppermute x22, waiting for transfers between devices, swap(): return lax.ppermute(values, 'ep', [(i, i ^ bits) for i in range(devices)])  27.7 us
    ppermute x22, starting transfers between devices, swap(): return lax.ppermute(values, 'ep', [(i, i ^ bits) for i in range(devices)])  19.4 us
    pallas_call x4, Pallas kernels, body(): keep, send = serve(me, column, other, *weights)  4.44 us
    pallas_call x1, Pallas kernels, body(): pl.pallas_call(load_kernel, out_shape=[jax.ShapeDtypeStruct(w.shape, w.dt...  2.88 us
  transfers between devices with their start and end apart: 22, of which 9 were waited for; matrix products, arithmetic and copies ran while one was open for 1% of the time, Pallas kernels for 13%

profile of v1, /device:TPU:0, one launch (start us, length us, event | category | flops | bytes accessed | tf_op | source)
XLA Modules:
  0.0 57.0 jit_solution(4859595236108007602)
XLA Ops:
  0.0 1.1 %pack_kernel.1 = bf16[32,2176]{1,0:T(8,128)(2,1)S(1)} custom-call(bf16[32,2048]{1,0:T(8,128)(2,1)} %refs_0_.2, s32[4,32]{1,0:T(4,128)} %bitcast.7, f32[4,32]{1,0:T(4,128)} %bitcast.8, f32[1,2048]{1,0:T(1,128)} %bitcast.6), custom_call_target="tpu_custom_call" | custom-call | tf_op jit(solution)/shard_map/pack_kernel/pallas_call | solution.py:124
  1.1 3.1 %collective-permute-start = (bf16[32,2176]{1,0:T(8,128)(2,1)S(1)}, bf16[32,2176]{1,0:T(8,128)(2,1)S(1)}, u32[]{:S(2)}, u32[]{:S(2)}) collective-permute-start(bf16[32,2176]{1,0:T(8,128)(2,1)S(1)} %pack_kernel.1), channel_id=1, source_target_pairs={{0,2},{1,3},{2,0},{3,1},{4,6},{5,7},{6,4},{7,5},{8,10},{9,11},{10,... | collective-permute-start | bytes 417800 | tf_op jit(solution)/shard_map/ppermute | solution.py:122
  4.2 2.6 %collective-permute-start.10 = (bf16[32,2176]{1,0:T(8,128)(2,1)S(1)}, bf16[32,2176]{1,0:T(8,128)(2,1)S(1)}, u32[]{:S(2)}, u32[]{:S(2)}) collective-permute-start(bf16[32,2176]{1,0:T(8,128)(2,1)S(1)} %pack_kernel.1), channel_id=1, source_target_pairs={{0,8},{1,9},{2,10},{3,11},{4,12},{5,13},{6,14},{7,15},{8,0},{9,1},... | collective-permute-start | bytes 417800 | tf_op jit(solution)/shard_map/ppermute | solution.py:122
  6.7 1.6 %collective-permute-start.4 = (bf16[32,2176]{1,0:T(8,128)(2,1)S(1)}, bf16[32,2176]{1,0:T(8,128)(2,1)S(1)}, u32[]{:S(2)}, u32[]{:S(2)}) collective-permute-start(bf16[32,2176]{1,0:T(8,128)(2,1)S(1)} %pack_kernel.1), channel_id=1, source_target_pairs={{0,4},{1,5},{2,6},{3,7},{4,0},{5,1},{6,2},{7,3},{8,12},{9,13},{10,... | collective-permute-start | bytes 417800 | tf_op jit(solution)/shard_map/ppermute | solution.py:122
  8.3 2.9 %load_kernel.1 = (bf16[1,2048,512]{2,1,0:T(8,128)(2,1)S(1)}, bf16[1,2048,512]{2,1,0:T(8,128)(2,1)S(1)}, bf16[1,512,2048]{2,1,0:T(8,128)(2,1)S(1)}) custom-call(bf16[1,2048,512]{2,1,0:T(8,128)(2,1)} %refs_0_.3, bf16[1,2048,512]{2,1,0:T(8,128)(2,1)} %refs_1_.1, bf16[1,512,2048]{2,1,0:T(8,128)(2,1)} %refs_2_.1), custom_call_target="tpu_custom_call" | custom-call | tf_op jit(solution)/shard_map/load_kernel/pallas_call | solution.py:144
  11.2 0.0 collective-permute-done
  11.2 0.1 collective-permute-start.1
  11.3 1.9 %collective-permute-done.10 = bf16[32,2176]{1,0:T(8,128)(2,1)S(1)} collective-permute-done((bf16[32,2176]{1,0:T(8,128)(2,1)S(1)}, bf16[32,2176]{1,0:T(8,128)(2,1)S(1)}, u32[]{:S(2)}, u32[]{:S(2)}) %collective-permute-start.10) | collective-permute-done | bytes 139296 | tf_op jit(solution)/shard_map/ppermute | solution.py:122
  13.3 0.6 %collective-permute-start.16 = (bf16[32,2176]{1,0:T(8,128)(2,1)S(1)}, bf16[32,2176]{1,0:T(8,128)(2,1)S(1)}, u32[]{:S(2)}, u32[]{:S(2)}) collective-permute-start(bf16[32,2176]{1,0:T(8,128)(2,1)S(1)} %collective-permute-done.10), channel_id=1, source_target_pairs={{0,4},{1,5},{2,6},{3,7},{4,0},{5,1},{6,2},{7,3},{8,12},{9,13},{10,... | collective-permute-start | bytes 417800 | tf_op jit(solution)/shard_map/ppermute | solution.py:122
  13.9 0.6 %collective-permute-start.11 = (bf16[32,2176]{1,0:T(8,128)(2,1)S(1)}, bf16[32,2176]{1,0:T(8,128)(2,1)S(1)}, u32[]{:S(2)}, u32[]{:S(2)}) collective-permute-start(bf16[32,2176]{1,0:T(8,128)(2,1)S(1)} %collective-permute-done.10), channel_id=1, source_target_pairs={{0,2},{1,3},{2,0},{3,1},{4,6},{5,7},{6,4},{7,5},{8,10},{9,11},{10,... | collective-permute-start | bytes 417800 | tf_op jit(solution)/shard_map/ppermute | solution.py:122
  14.4 0.0 collective-permute-done.4
  14.4 1.6 %collective-permute-start.5 = (bf16[32,2176]{1,0:T(8,128)(2,1)S(1)}, bf16[32,2176]{1,0:T(8,128)(2,1)S(1)}, u32[]{:S(2)}, u32[]{:S(2)}) collective-permute-start(bf16[32,2176]{1,0:T(8,128)(2,1)S(1)} %collective-permute-done.4), channel_id=1, source_target_pairs={{0,2},{1,3},{2,0},{3,1},{4,6},{5,7},{6,4},{7,5},{8,10},{9,11},{10,... | collective-permute-start | bytes 417800 | tf_op jit(solution)/shard_map/ppermute | solution.py:122
  16.0 4.4 %collective-permute-done.11 = bf16[32,2176]{1,0:T(8,128)(2,1)S(1)} collective-permute-done((bf16[32,2176]{1,0:T(8,128)(2,1)S(1)}, bf16[32,2176]{1,0:T(8,128)(2,1)S(1)}, u32[]{:S(2)}, u32[]{:S(2)}) %collective-permute-start.11) | collective-permute-done | bytes 139296 | tf_op jit(solution)/shard_map/ppermute | solution.py:122
  20.5 0.1 collective-permute-start.12
  20.6 1.7 %collective-permute-done.5 = bf16[32,2176]{1,0:T(8,128)(2,1)S(1)} collective-permute-done((bf16[32,2176]{1,0:T(8,128)(2,1)S(1)}, bf16[32,2176]{1,0:T(8,128)(2,1)S(1)}, u32[]{:S(2)}, u32[]{:S(2)}) %collective-permute-start.5) | collective-permute-done | bytes 139296 | tf_op jit(solution)/shard_map/ppermute | solution.py:122
  22.2 0.1 collective-permute-start.6
  22.3 0.0 collective-permute-done.16
  22.3 0.6 %collective-permute-start.17 = (bf16[32,2176]{1,0:T(8,128)(2,1)S(1)}, bf16[32,2176]{1,0:T(8,128)(2,1)S(1)}, u32[]{:S(2)}, u32[]{:S(2)}) collective-permute-start(bf16[32,2176]{1,0:T(8,128)(2,1)S(1)} %collective-permute-done.16), channel_id=1, source_target_pairs={{0,2},{1,3},{2,0},{3,1},{4,6},{5,7},{6,4},{7,5},{8,10},{9,11},{10,... | collective-permute-start | bytes 417800 | tf_op jit(solution)/shard_map/ppermute | solution.py:122
  22.9 0.0 collective-permute-done.1.refs_2_
  22.9 1.1 %expert_kernel.4 = (f32[64,2048]{1,0:T(8,128)S(1)}, bf16[64,2048]{1,0:T(8,128)(2,1)S(1)}) custom-call(s32[1]{0:T(128)} %bitcast.refs_0_, bf16[64,2176]{1,0:T(8,128)(2,1)S(1)} %pad_maximum_fusion.refs_1_, bf16[64,2176]{1,0:T(8,128)(2,1)S(1)} %collective-permute-done.1.refs_2_, bf16[1,2048,512]{2,1,0:T(8,128)(2,1)S(1)} %get-tuple-element.16.refs_3_, ...), custom_call_target="tpu_custom_call" | custom-call | tf_op jit(solution)/shard_map/expert_kernel/pallas_call | solution.py:168
  24.0 0.2 collective-permute-start.2
  24.3 4.1 %collective-permute-done.17 = bf16[32,2176]{1,0:T(8,128)(2,1)S(1)} collective-permute-done((bf16[32,2176]{1,0:T(8,128)(2,1)S(1)}, bf16[32,2176]{1,0:T(8,128)(2,1)S(1)}, u32[]{:S(2)}, u32[]{:S(2)}) %collective-permute-start.17) | collective-permute-done | bytes 139296 | tf_op jit(solution)/shard_map/ppermute | solution.py:122
  28.4 0.1 collective-permute-start.18
  28.5 0.0 collective-permute-done.12.refs_2_
  28.5 1.1 %expert_kernel.6 = (f32[64,2048]{1,0:T(8,128)S(1)}, bf16[64,2048]{1,0:T(8,128)(2,1)S(1)}) custom-call(s32[1]{0:T(128)} %bitcast.refs_0_, bf16[64,2176]{1,0:T(8,128)(2,1)S(1)} %constant_dynamic-update-slice_fusion.2.refs_1_, bf16[64,2176]{1,0:T(8,128)(2,1)S(1)} %collective-permute-done.12.refs_2_, bf16[1,2048,512]{2,1,0:T(8,128)(2,1)S(1)} %get-tuple-element.16.refs_3_, ...), custom_call_target="tpu_custom_call" | custom-call | tf_op jit(solution)/shard_map/expert_kernel/pallas_call | solution.py:168
  29.6 0.6 collective-permute-start.13
  30.2 0.0 collective-permute-done.6.refs_2_
  30.2 1.1 %expert_kernel.5 = (f32[64,2048]{1,0:T(8,128)S(1)}, bf16[64,2048]{1,0:T(8,128)(2,1)S(1)}) custom-call(s32[1]{0:T(128)} %bitcast.refs_0_, bf16[64,2176]{1,0:T(8,128)(2,1)S(1)} %constant_dynamic-update-slice_fusion.refs_1_, bf16[64,2176]{1,0:T(8,128)(2,1)S(1)} %collective-permute-done.6.refs_2_, bf16[1,2048,512]{2,1,0:T(8,128)(2,1)S(1)} %get-tuple-element.16.refs_3_, ...), custom_call_target="tpu_custom_call" | custom-call | tf_op jit(solution)/shard_map/expert_kernel/pallas_call | solution.py:168
  31.3 0.1 collective-permute-start.7
  31.4 0.0 collective-permute-done.2
  31.5 0.6 collective-permute-start.3
  32.0 0.0 collective-permute-done.18.refs_2_
  32.0 1.1 %expert_kernel.7 = (f32[64,2048]{1,0:T(8,128)S(1)}, bf16[64,2048]{1,0:T(8,128)(2,1)S(1)}) custom-call(s32[1]{0:T(128)} %bitcast.refs_0_, bf16[64,2176]{1,0:T(8,128)(2,1)S(1)} %constant_dynamic-update-slice_fusion.4.refs_1_, bf16[64,2176]{1,0:T(8,128)(2,1)S(1)} %collective-permute-done.18.refs_2_, bf16[1,2048,512]{2,1,0:T(8,128)(2,1)S(1)} %get-tuple-element.16.refs_3_, ...), custom_call_target="tpu_custom_call" | custom-call | tf_op jit(solution)/shard_map/expert_kernel/pallas_call | solution.py:168
  33.2 0.3 collective-permute-start.19
  33.4 0.0 collective-permute-done.13
  33.4 0.1 convert_add_fusion.1
  33.5 1.6 %collective-permute-start.14 = (bf16[32,2048]{1,0:T(8,128)(2,1)S(1)}, bf16[32,2048]{1,0:T(8,128)(2,1)S(1)}, u32[]{:S(2)}, u32[]{:S(2)}) collective-permute-start(bf16[32,2048]{1,0:T(8,128)(2,1)S(1)} %slice.59), channel_id=1, source_target_pairs={{0,2},{1,3},{2,0},{3,1},{4,6},{5,7},{6,4},{7,5},{8,10},{9,11},{10,... | collective-permute-start | bytes 393224 | tf_op jit(solution)/shard_map/ppermute | solution.py:122
  35.1 0.0 collective-permute-done.7
  35.2 0.0 copy-start
  35.2 0.6 %collective-permute-start.8 = (bf16[32,2048]{1,0:T(8,128)(2,1)S(1)}, bf16[32,2048]{1,0:T(8,128)(2,1)S(1)}, u32[]{:S(2)}, u32[]{:S(2)}) collective-permute-start(bf16[32,2048]{1,0:T(8,128)(2,1)S(1)} %slice.60), channel_id=1, source_target_pairs={{0,2},{1,3},{2,0},{3,1},{4,6},{5,7},{6,4},{7,5},{8,10},{9,11},{10,... | collective-permute-start | bytes 393224 | tf_op jit(solution)/shard_map/ppermute | solution.py:122
  35.8 4.9 %collective-permute-done.14 = bf16[32,2048]{1,0:T(8,128)(2,1)S(1)} collective-permute-done((bf16[32,2048]{1,0:T(8,128)(2,1)S(1)}, bf16[32,2048]{1,0:T(8,128)(2,1)S(1)}, u32[]{:S(2)}, u32[]{:S(2)}) %collective-permute-start.14) | collective-permute-done | bytes 131104 | tf_op jit(solution)/shard_map/ppermute | solution.py:122
  40.7 3.4 %collective-permute-start.15 = (bf16[32,2048]{1,0:T(8,128)(2,1)S(1)}, bf16[32,2048]{1,0:T(8,128)(2,1)S(1)}, u32[]{:S(2)}, u32[]{:S(2)}) collective-permute-start(bf16[32,2048]{1,0:T(8,128)(2,1)S(1)} %fusion.1), channel_id=1, source_target_pairs={{0,8},{1,9},{2,10},{3,11},{4,12},{5,13},{6,14},{7,15},{8,0},{9,1},... | collective-permute-start | bytes 393224 | tf_op jit(solution)/shard_map/ppermute | solution.py:122
  44.2 0.0 collective-permute-done.19
  44.2 0.1 convert_add_fusion
  44.3 0.8 %collective-permute-start.20 = (bf16[32,2048]{1,0:T(8,128)(2,1)S(1)}, bf16[32,2048]{1,0:T(8,128)(2,1)S(1)}, u32[]{:S(2)}, u32[]{:S(2)}) collective-permute-start(bf16[32,2048]{1,0:T(8,128)(2,1)S(1)} %slice.58), channel_id=1, source_target_pairs={{0,2},{1,3},{2,0},{3,1},{4,6},{5,7},{6,4},{7,5},{8,10},{9,11},{10,... | collective-permute-start | bytes 393224 | tf_op jit(solution)/shard_map/ppermute | solution.py:122
  45.1 0.0 collective-permute-done.8
  45.1 0.3 collective-permute-start.9
  45.5 3.8 %collective-permute-done.20 = bf16[32,2048]{1,0:T(8,128)(2,1)S(1)} collective-permute-done((bf16[32,2048]{1,0:T(8,128)(2,1)S(1)}, bf16[32,2048]{1,0:T(8,128)(2,1)S(1)}, u32[]{:S(2)}, u32[]{:S(2)}) %collective-permute-start.20) | collective-permute-done | bytes 131104 | tf_op jit(solution)/shard_map/ppermute | solution.py:122
  49.3 0.1 collective-permute-start.21
  49.4 0.0 collective-permute-done.3
  49.5 0.2 collective-permute-done.15.refs_2_
  49.6 1.9 %collective-permute-done.9.refs_1_ = bf16[32,2048]{1,0:T(8,128)(2,1)S(1)} collective-permute-done((bf16[32,2048]{1,0:T(8,128)(2,1)S(1)}, bf16[32,2048]{1,0:T(8,128)(2,1)S(1)}, u32[]{:S(2)}, u32[]{:S(2)}) %collective-permute-start.9) | collective-permute-done | bytes 131104 | tf_op jit(solution)/shard_map/ppermute | solution.py:122
  51.5 4.7 %collective-permute-done.21.refs_3_ = bf16[32,2048]{1,0:T(8,128)(2,1)S(1)} collective-permute-done((bf16[32,2048]{1,0:T(8,128)(2,1)S(1)}, bf16[32,2048]{1,0:T(8,128)(2,1)S(1)}, u32[]{:S(2)}, u32[]{:S(2)}) %collective-permute-start.21) | collective-permute-done | bytes 131104 | tf_op jit(solution)/shard_map/ppermute | solution.py:122
  56.2 0.0 copy-done
  56.2 0.8 %finish_kernel.1 = bf16[32,2048]{1,0:T(8,128)(2,1)} custom-call(f32[32,2048]{1,0:T(8,128)S(1)} %slice_add_fusion.3.refs_0_, bf16[32,2048]{1,0:T(8,128)(2,1)S(1)} %collective-permute-done.9.refs_1_, bf16[32,2048]{1,0:T(8,128)(2,1)S(1)} %collective-permute-done.15.refs_2_, bf16[32,2048]{1,0:T(8,128)(2,1)S(1)} %collective-permute-done.21.refs_3_, ...), custom_call_target="tpu_custom_call" | custom-call | tf_op jit(solution)/shard_map/finish_kernel/pallas_call | solution.py:173
  (17 shorter events, 0.4 us)
Async XLA Ops:
  1.1 10.1 %collective-permute-start = (bf16[32,2176]{1,0:T(8,128)(2,1)S(1)}, bf16[32,2176]{1,0:T(8,128)(2,1)S(1)}, u32[]{:S(2)}, u32[]{:S(2)}) collective-permute-start(bf16[32,2176]{1,0:T(8,128)(2,1)S(1)} %pack_kernel.1), channel_id=1, source_target_pairs={{0,2},{1,3},{2,0},{3,1},{4,6},{5,7},{6,4},{7,5},{8,10},{9,11},{10,... | collective-permute-start | bytes 417800 | tf_op jit(solution)/shard_map/ppermute | solution.py:122
  4.2 9.1 %collective-permute-start.10 = (bf16[32,2176]{1,0:T(8,128)(2,1)S(1)}, bf16[32,2176]{1,0:T(8,128)(2,1)S(1)}, u32[]{:S(2)}, u32[]{:S(2)}) collective-permute-start(bf16[32,2176]{1,0:T(8,128)(2,1)S(1)} %pack_kernel.1), channel_id=1, source_target_pairs={{0,8},{1,9},{2,10},{3,11},{4,12},{5,13},{6,14},{7,15},{8,0},{9,1},... | collective-permute-start | bytes 417800 | tf_op jit(solution)/shard_map/ppermute | solution.py:122
  6.7 7.7 %collective-permute-start.4 = (bf16[32,2176]{1,0:T(8,128)(2,1)S(1)}, bf16[32,2176]{1,0:T(8,128)(2,1)S(1)}, u32[]{:S(2)}, u32[]{:S(2)}) collective-permute-start(bf16[32,2176]{1,0:T(8,128)(2,1)S(1)} %pack_kernel.1), channel_id=1, source_target_pairs={{0,4},{1,5},{2,6},{3,7},{4,0},{5,1},{6,2},{7,3},{8,12},{9,13},{10,... | collective-permute-start | bytes 417800 | tf_op jit(solution)/shard_map/ppermute | solution.py:122
  11.2 11.7 %collective-permute-start.1 = (bf16[64,2176]{1,0:T(8,128)(2,1)S(1)}, bf16[64,2176]{1,0:T(8,128)(2,1)S(1)}, u32[]{:S(2)}, u32[]{:S(2)}) collective-permute-start(bf16[64,2176]{1,0:T(8,128)(2,1)S(1)} %pad_maximum_fusion.refs_1_), channel_id=1, source_target_pairs={{0,1},{1,0},{2,3},{3,2},{4,5},{5,4},{6,7},{7,6},{8,9},{9,8},{10,11... | collective-permute-start | bytes 835592 | tf_op jit(solution)/shard_map/ppermute | solution.py:122
  13.3 9.1 %collective-permute-start.16 = (bf16[32,2176]{1,0:T(8,128)(2,1)S(1)}, bf16[32,2176]{1,0:T(8,128)(2,1)S(1)}, u32[]{:S(2)}, u32[]{:S(2)}) collective-permute-start(bf16[32,2176]{1,0:T(8,128)(2,1)S(1)} %collective-permute-done.10), channel_id=1, source_target_pairs={{0,4},{1,5},{2,6},{3,7},{4,0},{5,1},{6,2},{7,3},{8,12},{9,13},{10,... | collective-permute-start | bytes 417800 | tf_op jit(solution)/shard_map/ppermute | solution.py:122
  13.9 6.6 %collective-permute-start.11 = (bf16[32,2176]{1,0:T(8,128)(2,1)S(1)}, bf16[32,2176]{1,0:T(8,128)(2,1)S(1)}, u32[]{:S(2)}, u32[]{:S(2)}) collective-permute-start(bf16[32,2176]{1,0:T(8,128)(2,1)S(1)} %collective-permute-done.10), channel_id=1, source_target_pairs={{0,2},{1,3},{2,0},{3,1},{4,6},{5,7},{6,4},{7,5},{8,10},{9,11},{10,... | collective-permute-start | bytes 417800 | tf_op jit(solution)/shard_map/ppermute | solution.py:122
  14.4 7.8 %collective-permute-start.5 = (bf16[32,2176]{1,0:T(8,128)(2,1)S(1)}, bf16[32,2176]{1,0:T(8,128)(2,1)S(1)}, u32[]{:S(2)}, u32[]{:S(2)}) collective-permute-start(bf16[32,2176]{1,0:T(8,128)(2,1)S(1)} %collective-permute-done.4), channel_id=1, source_target_pairs={{0,2},{1,3},{2,0},{3,1},{4,6},{5,7},{6,4},{7,5},{8,10},{9,11},{10,... | collective-permute-start | bytes 417800 | tf_op jit(solution)/shard_map/ppermute | solution.py:122
  20.5 8.0 %collective-permute-start.12 = (bf16[64,2176]{1,0:T(8,128)(2,1)S(1)}, bf16[64,2176]{1,0:T(8,128)(2,1)S(1)}, u32[]{:S(2)}, u32[]{:S(2)}) collective-permute-start(bf16[64,2176]{1,0:T(8,128)(2,1)S(1)} %constant_dynamic-update-slice_fusion.2.refs_1_), channel_id=1, source_target_pairs={{0,1},{1,0},{2,3},{3,2},{4,5},{5,4},{6,7},{7,6},{8,9},{9,8},{10,11... | collective-permute-start | bytes 835592 | tf_op jit(solution)/shard_map/ppermute | solution.py:122
  22.2 7.9 %collective-permute-start.6 = (bf16[64,2176]{1,0:T(8,128)(2,1)S(1)}, bf16[64,2176]{1,0:T(8,128)(2,1)S(1)}, u32[]{:S(2)}, u32[]{:S(2)}) collective-permute-start(bf16[64,2176]{1,0:T(8,128)(2,1)S(1)} %constant_dynamic-update-slice_fusion.refs_1_), channel_id=1, source_target_pairs={{0,1},{1,0},{2,3},{3,2},{4,5},{5,4},{6,7},{7,6},{8,9},{9,8},{10,11... | collective-permute-start | bytes 835592 | tf_op jit(solution)/shard_map/ppermute | solution.py:122
  22.3 6.1 %collective-permute-start.17 = (bf16[32,2176]{1,0:T(8,128)(2,1)S(1)}, bf16[32,2176]{1,0:T(8,128)(2,1)S(1)}, u32[]{:S(2)}, u32[]{:S(2)}) collective-permute-start(bf16[32,2176]{1,0:T(8,128)(2,1)S(1)} %collective-permute-done.16), channel_id=1, source_target_pairs={{0,2},{1,3},{2,0},{3,1},{4,6},{5,7},{6,4},{7,5},{8,10},{9,11},{10,... | collective-permute-start | bytes 417800 | tf_op jit(solution)/shard_map/ppermute | solution.py:122
  24.0 7.3 %collective-permute-start.2 = (bf16[64,2048]{1,0:T(8,128)(2,1)S(1)}, bf16[64,2048]{1,0:T(8,128)(2,1)S(1)}, u32[]{:S(2)}, u32[]{:S(2)}) collective-permute-start(bf16[64,2048]{1,0:T(8,128)(2,1)S(1)} %get-tuple-element.20), channel_id=1, source_target_pairs={{0,1},{1,0},{2,3},{3,2},{4,5},{5,4},{6,7},{7,6},{8,9},{9,8},{10,11... | collective-permute-start | bytes 786440 | tf_op jit(solution)/shard_map/ppermute | solution.py:122
  28.4 3.6 %collective-permute-start.18 = (bf16[64,2176]{1,0:T(8,128)(2,1)S(1)}, bf16[64,2176]{1,0:T(8,128)(2,1)S(1)}, u32[]{:S(2)}, u32[]{:S(2)}) collective-permute-start(bf16[64,2176]{1,0:T(8,128)(2,1)S(1)} %constant_dynamic-update-slice_fusion.4.refs_1_), channel_id=1, source_target_pairs={{0,1},{1,0},{2,3},{3,2},{4,5},{5,4},{6,7},{7,6},{8,9},{9,8},{10,11... | collective-permute-start | bytes 835592 | tf_op jit(solution)/shard_map/ppermute | solution.py:122
  29.6 3.8 %collective-permute-start.13 = (bf16[64,2048]{1,0:T(8,128)(2,1)S(1)}, bf16[64,2048]{1,0:T(8,128)(2,1)S(1)}, u32[]{:S(2)}, u32[]{:S(2)}) collective-permute-start(bf16[64,2048]{1,0:T(8,128)(2,1)S(1)} %get-tuple-element.24), channel_id=1, source_target_pairs={{0,1},{1,0},{2,3},{3,2},{4,5},{5,4},{6,7},{7,6},{8,9},{9,8},{10,11... | collective-permute-start | bytes 786440 | tf_op jit(solution)/shard_map/ppermute | solution.py:122
  31.3 3.8 %collective-permute-start.7 = (bf16[64,2048]{1,0:T(8,128)(2,1)S(1)}, bf16[64,2048]{1,0:T(8,128)(2,1)S(1)}, u32[]{:S(2)}, u32[]{:S(2)}) collective-permute-start(bf16[64,2048]{1,0:T(8,128)(2,1)S(1)} %get-tuple-element.22), channel_id=1, source_target_pairs={{0,1},{1,0},{2,3},{3,2},{4,5},{5,4},{6,7},{7,6},{8,9},{9,8},{10,11... | collective-permute-start | bytes 786440 | tf_op jit(solution)/shard_map/ppermute | solution.py:122
  31.5 18.0 %collective-permute-start.3 = (bf16[32,2048]{1,0:T(8,128)(2,1)S(1)}, bf16[32,2048]{1,0:T(8,128)(2,1)S(1)}, u32[]{:S(2)}, u32[]{:S(2)}) collective-permute-start(bf16[32,2048]{1,0:T(8,128)(2,1)S(1)} %slice.61), channel_id=1, source_target_pairs={{0,2},{1,3},{2,0},{3,1},{4,6},{5,7},{6,4},{7,5},{8,10},{9,11},{10,... | collective-permute-start | bytes 393224 | tf_op jit(solution)/shard_map/ppermute | solution.py:122
  33.2 11.0 %collective-permute-start.19 = (bf16[64,2048]{1,0:T(8,128)(2,1)S(1)}, bf16[64,2048]{1,0:T(8,128)(2,1)S(1)}, u32[]{:S(2)}, u32[]{:S(2)}) collective-permute-start(bf16[64,2048]{1,0:T(8,128)(2,1)S(1)} %get-tuple-element.26), channel_id=1, source_target_pairs={{0,1},{1,0},{2,3},{3,2},{4,5},{5,4},{6,7},{7,6},{8,9},{9,8},{10,11... | collective-permute-start | bytes 786440 | tf_op jit(solution)/shard_map/ppermute | solution.py:122
  33.5 7.2 %collective-permute-start.14 = (bf16[32,2048]{1,0:T(8,128)(2,1)S(1)}, bf16[32,2048]{1,0:T(8,128)(2,1)S(1)}, u32[]{:S(2)}, u32[]{:S(2)}) collective-permute-start(bf16[32,2048]{1,0:T(8,128)(2,1)S(1)} %slice.59), channel_id=1, source_target_pairs={{0,2},{1,3},{2,0},{3,1},{4,6},{5,7},{6,4},{7,5},{8,10},{9,11},{10,... | collective-permute-start | bytes 393224 | tf_op jit(solution)/shard_map/ppermute | solution.py:122
  35.2 21.0 %copy-start = (f32[2048]{0:T(1024)S(1)}, f32[2048]{0:T(1024)}, u32[]{:S(2)}) copy-start(f32[2048]{0:T(1024)} %param.15) | copy-start | bytes 24580
  35.2 9.9 %collective-permute-start.8 = (bf16[32,2048]{1,0:T(8,128)(2,1)S(1)}, bf16[32,2048]{1,0:T(8,128)(2,1)S(1)}, u32[]{:S(2)}, u32[]{:S(2)}) collective-permute-start(bf16[32,2048]{1,0:T(8,128)(2,1)S(1)} %slice.60), channel_id=1, source_target_pairs={{0,2},{1,3},{2,0},{3,1},{4,6},{5,7},{6,4},{7,5},{8,10},{9,11},{10,... | collective-permute-start | bytes 393224 | tf_op jit(solution)/shard_map/ppermute | solution.py:122
  40.7 8.9 %collective-permute-start.15 = (bf16[32,2048]{1,0:T(8,128)(2,1)S(1)}, bf16[32,2048]{1,0:T(8,128)(2,1)S(1)}, u32[]{:S(2)}, u32[]{:S(2)}) collective-permute-start(bf16[32,2048]{1,0:T(8,128)(2,1)S(1)} %fusion.1), channel_id=1, source_target_pairs={{0,8},{1,9},{2,10},{3,11},{4,12},{5,13},{6,14},{7,15},{8,0},{9,1},... | collective-permute-start | bytes 393224 | tf_op jit(solution)/shard_map/ppermute | solution.py:122
  44.3 5.0 %collective-permute-start.20 = (bf16[32,2048]{1,0:T(8,128)(2,1)S(1)}, bf16[32,2048]{1,0:T(8,128)(2,1)S(1)}, u32[]{:S(2)}, u32[]{:S(2)}) collective-permute-start(bf16[32,2048]{1,0:T(8,128)(2,1)S(1)} %slice.58), channel_id=1, source_target_pairs={{0,2},{1,3},{2,0},{3,1},{4,6},{5,7},{6,4},{7,5},{8,10},{9,11},{10,... | collective-permute-start | bytes 393224 | tf_op jit(solution)/shard_map/ppermute | solution.py:122
  45.1 6.4 %collective-permute-start.9 = (bf16[32,2048]{1,0:T(8,128)(2,1)S(1)}, bf16[32,2048]{1,0:T(8,128)(2,1)S(1)}, u32[]{:S(2)}, u32[]{:S(2)}) collective-permute-start(bf16[32,2048]{1,0:T(8,128)(2,1)S(1)} %fusion.2), channel_id=1, source_target_pairs={{0,4},{1,5},{2,6},{3,7},{4,0},{5,1},{6,2},{7,3},{8,12},{9,13},{10,... | collective-permute-start | bytes 393224 | tf_op jit(solution)/shard_map/ppermute | solution.py:122
  49.3 6.8 %collective-permute-start.21 = (bf16[32,2048]{1,0:T(8,128)(2,1)S(1)}, bf16[32,2048]{1,0:T(8,128)(2,1)S(1)}, u32[]{:S(2)}, u32[]{:S(2)}) collective-permute-start(bf16[32,2048]{1,0:T(8,128)(2,1)S(1)} %fusion), channel_id=1, source_target_pairs={{0,12},{1,13},{2,14},{3,15},{4,8},{5,9},{6,10},{7,11},{8,4},{9,5},... | collective-permute-start | bytes 393224 | tf_op jit(solution)/shard_map/ppermute | solution.py:122

commit v2 on v1

--- a/solution.py
+++ b/solution.py
@@ -8,10 +8,11 @@
 epsilon = 1e-06
 QUAD = 4
 PARTS = 3
+MERGE = 2
 
 
 def pack_kernel(
-    tokens_hbm, routing_hbm, weights_hbm, gain_hbm, out_ref, tokens_ref, routing_ref, weights_ref,
+    me_ref, tokens_hbm, routing_hbm, weights_hbm, gain_hbm, out_ref, place_ref, tokens_ref, routing_ref, weights_ref,
     gain_ref, sems, *, experts, extra
 ):
     copies = [
@@ -29,6 +30,7 @@
         copy.start()
     for copy in copies:
         copy.wait()
+    place_ref[...] = jnp.full(place_ref.shape, me_ref[0], jnp.int32)
     rows, width = tokens_ref.shape
     floats = tokens_ref[...].astype(jnp.float32)
     scale = lax.rsqrt(jnp.mean(floats * floats, axis=-1, keepdims=True) + epsilon)
@@ -69,23 +71,28 @@
         copy.wait()
 
 
-def expert_kernel(
-    me_ref, mine_ref, other_ref, gate_ref, up_ref, down_ref, keep_ref, send_ref, *, experts
-):
-    rows, _ = mine_ref.shape
-    width = gate_ref.shape[1]
-    both = jnp.concatenate([mine_ref[...], other_ref[...]], axis=0)
+def expert_kernel(*refs, experts, count):
+    place_ref, blocks, rest = refs[0], refs[1 : 1 + 2 * count], refs[1 + 2 * count :]
+    weights, outs = rest[:6], rest[6:]
+    rows, width = outs[0].shape
+    both = jnp.concatenate([block[...] for block in blocks], axis=0)
     values = both[:, :width]
     table = both[:, width:].astype(jnp.float32)
     lane = lax.broadcasted_iota(jnp.int32, table.shape, 1)
-    chosen = (lane % experts == me_ref[0]) & (lane < PARTS * experts)
-    weight = jnp.sum(jnp.where(chosen, table, 0.0), axis=1, keepdims=True)
-    gate = jnp.dot(values, gate_ref[0], preferred_element_type=jnp.float32)
-    upward = jnp.dot(values, up_ref[0], preferred_element_type=jnp.float32)
-    hidden = (gate / (1.0 + jnp.exp(-gate)) * upward).astype(jnp.bfloat16)
-    served = jnp.dot(hidden, down_ref[0], preferred_element_type=jnp.float32) * weight
-    keep_ref[...] = served[:rows]
-    send_ref[...] = served[rows:].astype(jnp.bfloat16)
+    total = None
+    for bit, (gate_ref, up_ref, down_ref) in enumerate((weights[:3], weights[3:])):
+        chosen = (lane % experts == (place_ref[:, :1] ^ bit)) & (lane < PARTS * experts)
+        weight = jnp.sum(jnp.where(chosen, table, 0.0), axis=1, keepdims=True)
+        gate = jnp.dot(values, gate_ref[0], preferred_element_type=jnp.float32)
+        upward = jnp.dot(values, up_ref[0], preferred_element_type=jnp.float32)
+        hidden = (gate / (1.0 + jnp.exp(-gate)) * upward).astype(jnp.bfloat16)
+        served = jnp.dot(hidden, down_ref[0], preferred_element_type=jnp.float32) * weight
+        total = served if total is None else total + served
+    for i in range(count):
+        outs[i][...] = total[i * rows : (i + 1) * rows]
+        outs[count + i][...] = total[(count + i) * rows : (count + i + 1) * rows].astype(
+            jnp.bfloat16
+        )
 
 
 def finish_kernel(*refs):
@@ -110,10 +117,15 @@
     return j & -j
 
 
+def groups_of(slabs):
+    first = min(MERGE, slabs)
+    return {0: tuple(range(first))} | {j: (j,) for j in range(first, slabs)}
+
+
 def body(tokens, routing, gate_weights, pre_gain, w_gate, w_up, w_down, post_gain):
     rows, width = tokens.shape
+    devices = lax.axis_size("ep")
     choices = routing.shape[1]
-    devices = lax.axis_size("ep")
     extra = -(-PARTS * devices // 128) * 128
     slabs = devices // QUAD
     me = lax.axis_index("ep").astype(jnp.int32).reshape(1)
@@ -121,11 +133,14 @@
     def swap(values, bits):
         return lax.ppermute(values, "ep", [(i, i ^ bits) for i in range(devices)])
 
-    packed = pl.pallas_call(
+    packed, place = pl.pallas_call(
         lambda *refs: pack_kernel(*refs, experts=devices, extra=extra),
-        out_shape=jax.ShapeDtypeStruct((rows, width + extra), jnp.bfloat16),
-        in_specs=[IN_HBM] * 4,
-        out_specs=IN_VMEM,
+        out_shape=(
+            jax.ShapeDtypeStruct((rows, width + extra), jnp.bfloat16),
+            jax.ShapeDtypeStruct((1, 128), jnp.int32),
+        ),
+        in_specs=[IN_SMEM] + [IN_HBM] * 4,
+        out_specs=(IN_VMEM, IN_VMEM),
         scratch_shapes=[
             pltpu.VMEM((rows, width), tokens.dtype),
             pltpu.VMEM((choices, rows), routing.dtype),
@@ -135,7 +150,7 @@
         ],
         name="pack_kernel",
         compiler_params=pltpu.CompilerParams(vmem_limit_bytes=4 << 20),
-    )(*map(in_hbm, (tokens, routing.T, gate_weights.T, pre_gain.reshape(1, width))))
+    )(me, *map(in_hbm, (tokens, routing.T, gate_weights.T, pre_gain.reshape(1, width))))
 
     blocks = {0: packed}
     for j in range(1, slabs):
@@ -151,25 +166,23 @@
         compiler_params=pltpu.CompilerParams(vmem_limit_bytes=4 << 20),
     )(*map(in_hbm, (w_gate, w_up, w_down)))
 
-    serve = pl.pallas_call(
-        lambda *refs: expert_kernel(*refs, experts=devices),
-        out_shape=(
-            jax.ShapeDtypeStruct((2 * rows, width), jnp.float32),
-            jax.ShapeDtypeStruct((2 * rows, width), jnp.bfloat16),
-        ),
-        in_specs=[IN_SMEM] + [IN_VMEM] * 5,
-        name="expert_kernel",
-        compiler_params=pltpu.CompilerParams(vmem_limit_bytes=16 << 20),
-    )
+    weights = [*weights] + [swap(w, 1) for w in (w_gate, w_up, w_down)]
+
+    across = {j: swap(blocks[j], 2) for j in range(slabs)}
     home = {}
-    for j in range(slabs):
-        column = jnp.concatenate([blocks[j], swap(blocks[j], 2)], axis=0)
-        other = swap(column, 1)
-        keep, send = serve(me, column, other, *weights)
-        column = keep + swap(send, 1).astype(jnp.float32)
-        back = swap(column[rows:].astype(jnp.bfloat16), 2)
-        total = column[:rows] + back.astype(jnp.float32)
-        home[j] = total if j == 0 else swap(total.astype(jnp.bfloat16), QUAD * j)
+    for members in groups_of(slabs).values():
+        count = len(members)
+        served = pl.pallas_call(
+            lambda *refs: expert_kernel(*refs, experts=devices, count=count),
+            out_shape=[jax.ShapeDtypeStruct((rows, width), jnp.float32)] * count
+            + [jax.ShapeDtypeStruct((rows, width), jnp.bfloat16)] * count,
+            in_specs=[IN_VMEM] * (7 + 2 * count),
+            name="expert_kernel",
+            compiler_params=pltpu.CompilerParams(vmem_limit_bytes=20 << 20),
+        )(place, *[blocks[j] for j in members], *[across[j] for j in members], *weights)
+        for j, keep, send in zip(members, served[:count], served[count:]):
+            total = keep + swap(send, 2).astype(jnp.float32)
+            home[j] = swap(total.astype(jnp.bfloat16), QUAD * j) if j else total
     return pl.pallas_call(
         finish_kernel,
         out_shape=jax.ShapeDtypeStruct((rows, width), jnp.bfloat16),

time: 57.2 us -> 57.8 us (1.010)
  Pallas kernels: 9.22 us -> 18.4 us
  waiting for transfers between devices: 27.7 us -> 19.2 us
    pallas_call x4 -> x3, Pallas kernels: 4.44 us -> 13.6 us  [body(): pl.pallas_call(lambda *refs: expert_kernel(*refs, experts=devices, count=...]
    ppermute x22 -> x17, waiting for transfers between devices: 27.7 us -> 19.2 us  [swap(): return lax.ppermute(values, 'ep', [(i, i ^ bits) for i in range(devices)])]
    ppermute x22 -> x17, starting transfers between devices: 19.4 us -> 19.8 us  [swap(): return lax.ppermute(values, 'ep', [(i, i ^ bits) for i in range(devices)])]
  transfers between devices with their start and end apart: 22 -> 17, of which waited for: 9 -> 9; matrix products, arithmetic and copies ran while one was open for 1% -> 0% of each run, Pallas kernels for 13% -> 30%
where the time goes in v2:
time: 57.8 us; the launch traced here: 57.6 us
  starting transfers between devices  19.8 us (34%)
  waiting for transfers between devices  19.2 us (33%)
  Pallas kernels  18.4 us (32%)
    ppermute x17, starting transfers between devices, swap(): return lax.ppermute(values, 'ep', [(i, i ^ bits) for i in range(devices)])  19.8 us
    ppermute x17, waiting for transfers between devices, swap(): return lax.ppermute(values, 'ep', [(i, i ^ bits) for i in range(devices)])  19.2 us
    pallas_call x3, Pallas kernels, body(): pl.pallas_call(lambda *refs: expert_kernel(*refs, experts=devices, count=...  13.6 us
    pallas_call x1, Pallas kernels, body(): pl.pallas_call(load_kernel, out_shape=[jax.ShapeDtypeStruct(w.shape, w.dt...  2.88 us
  transfers between devices with their start and end apart: 17, of which 9 were waited for; matrix products, arithmetic and copies ran while one was open for 0% of the time, Pallas kernels for 30%

profile of v2, /device:TPU:0, one launch (start us, length us, event | category | flops | bytes accessed | tf_op | source)
XLA Modules:
  0.0 57.6 jit_solution(14710610363994512191)
XLA Ops:
  0.0 0.5 collective-permute-start.3
  0.5 0.0 collective-permute-start.4
  0.5 0.5 collective-permute-start.5
  1.0 1.1 %pack_kernel.1 = (bf16[32,2176]{1,0:T(8,128)(2,1)S(1)}, s32[1,128]{1,0:T(1,128)S(1)}) custom-call(s32[1]{0:T(128)} %bitcast.refs_0_, bf16[32,2048]{1,0:T(8,128)(2,1)} %refs_1_.2, s32[4,32]{1,0:T(4,128)} %bitcast.7, f32[4,32]{1,0:T(4,128)} %bitcast.8, f32[1,2048]{1,0:T(1,128)} %bitcast.6), custom_call_target="tpu_custom_call" | custom-call | tf_op jit(solution)/shard_map/pack_kernel/pallas_call | solution.py:136
  2.1 2.6 %collective-permute-start = (bf16[32,2176]{1,0:T(8,128)(2,1)S(1)}, bf16[32,2176]{1,0:T(8,128)(2,1)S(1)}, u32[]{:S(2)}, u32[]{:S(2)}) collective-permute-start(bf16[32,2176]{1,0:T(8,128)(2,1)S(1)} %get-tuple-element.19.refs_1_), channel_id=1, source_target_pairs={{0,4},{1,5},{2,6},{3,7},{4,0},{5,1},{6,2},{7,3},{8,12},{9,13},{10,... | collective-permute-start | bytes 417800 | tf_op jit(solution)/shard_map/ppermute | solution.py:134
  4.7 2.6 %collective-permute-start.9 = (bf16[32,2176]{1,0:T(8,128)(2,1)S(1)}, bf16[32,2176]{1,0:T(8,128)(2,1)S(1)}, u32[]{:S(2)}, u32[]{:S(2)}) collective-permute-start(bf16[32,2176]{1,0:T(8,128)(2,1)S(1)} %get-tuple-element.19.refs_1_), channel_id=1, source_target_pairs={{0,8},{1,9},{2,10},{3,11},{4,12},{5,13},{6,14},{7,15},{8,0},{9,1},... | collective-permute-start | bytes 417800 | tf_op jit(solution)/shard_map/ppermute | solution.py:134
  7.3 4.6 %collective-permute-done.refs_2_ = bf16[32,2176]{1,0:T(8,128)(2,1)S(1)} collective-permute-done((bf16[32,2176]{1,0:T(8,128)(2,1)S(1)}, bf16[32,2176]{1,0:T(8,128)(2,1)S(1)}, u32[]{:S(2)}, u32[]{:S(2)}) %collective-permute-start) | collective-permute-done | bytes 139296 | tf_op jit(solution)/shard_map/ppermute | solution.py:134
  11.9 1.7 %collective-permute-start.1 = (bf16[32,2176]{1,0:T(8,128)(2,1)S(1)}, bf16[32,2176]{1,0:T(8,128)(2,1)S(1)}, u32[]{:S(2)}, u32[]{:S(2)}) collective-permute-start(bf16[32,2176]{1,0:T(8,128)(2,1)S(1)} %get-tuple-element.19.refs_1_), channel_id=1, source_target_pairs={{0,2},{1,3},{2,0},{3,1},{4,6},{5,7},{6,4},{7,5},{8,10},{9,11},{10,... | collective-permute-start | bytes 417800 | tf_op jit(solution)/shard_map/ppermute | solution.py:134
  13.6 0.8 %collective-permute-done.9.refs_1_ = bf16[32,2176]{1,0:T(8,128)(2,1)S(1)} collective-permute-done((bf16[32,2176]{1,0:T(8,128)(2,1)S(1)}, bf16[32,2176]{1,0:T(8,128)(2,1)S(1)}, u32[]{:S(2)}, u32[]{:S(2)}) %collective-permute-start.9) | collective-permute-done | bytes 139296 | tf_op jit(solution)/shard_map/ppermute | solution.py:134
  14.5 0.4 collective-permute-start.13
  14.9 2.4 %collective-permute-done.1.refs_3_ = bf16[32,2176]{1,0:T(8,128)(2,1)S(1)} collective-permute-done((bf16[32,2176]{1,0:T(8,128)(2,1)S(1)}, bf16[32,2176]{1,0:T(8,128)(2,1)S(1)}, u32[]{:S(2)}, u32[]{:S(2)}) %collective-permute-start.1) | collective-permute-done | bytes 139296 | tf_op jit(solution)/shard_map/ppermute | solution.py:134
  17.3 1.4 %collective-permute-start.2 = (bf16[32,2176]{1,0:T(8,128)(2,1)S(1)}, bf16[32,2176]{1,0:T(8,128)(2,1)S(1)}, u32[]{:S(2)}, u32[]{:S(2)}) collective-permute-start(bf16[32,2176]{1,0:T(8,128)(2,1)S(1)} %collective-permute-done.refs_2_), channel_id=1, source_target_pairs={{0,2},{1,3},{2,0},{3,1},{4,6},{5,7},{6,4},{7,5},{8,10},{9,11},{10,... | collective-permute-start | bytes 417800 | tf_op jit(solution)/shard_map/ppermute | solution.py:134
  18.7 0.8 %collective-permute-done.13.refs_1_ = bf16[32,2176]{1,0:T(8,128)(2,1)S(1)} collective-permute-done((bf16[32,2176]{1,0:T(8,128)(2,1)S(1)}, bf16[32,2176]{1,0:T(8,128)(2,1)S(1)}, u32[]{:S(2)}, u32[]{:S(2)}) %collective-permute-start.13) | collective-permute-done | bytes 139296 | tf_op jit(solution)/shard_map/ppermute | solution.py:134
  19.5 1.5 %collective-permute-start.14 = (bf16[32,2176]{1,0:T(8,128)(2,1)S(1)}, bf16[32,2176]{1,0:T(8,128)(2,1)S(1)}, u32[]{:S(2)}, u32[]{:S(2)}) collective-permute-start(bf16[32,2176]{1,0:T(8,128)(2,1)S(1)} %collective-permute-done.13.refs_1_), channel_id=1, source_target_pairs={{0,2},{1,3},{2,0},{3,1},{4,6},{5,7},{6,4},{7,5},{8,10},{9,11},{10,... | collective-permute-start | bytes 417800 | tf_op jit(solution)/shard_map/ppermute | solution.py:134
  21.0 2.8 %collective-permute-done.2.refs_4_ = bf16[32,2176]{1,0:T(8,128)(2,1)S(1)} collective-permute-done((bf16[32,2176]{1,0:T(8,128)(2,1)S(1)}, bf16[32,2176]{1,0:T(8,128)(2,1)S(1)}, u32[]{:S(2)}, u32[]{:S(2)}) %collective-permute-start.2) | collective-permute-done | bytes 139296 | tf_op jit(solution)/shard_map/ppermute | solution.py:134
  23.8 0.6 %collective-permute-start.10 = (bf16[32,2176]{1,0:T(8,128)(2,1)S(1)}, bf16[32,2176]{1,0:T(8,128)(2,1)S(1)}, u32[]{:S(2)}, u32[]{:S(2)}) collective-permute-start(bf16[32,2176]{1,0:T(8,128)(2,1)S(1)} %collective-permute-done.9.refs_1_), channel_id=1, source_target_pairs={{0,2},{1,3},{2,0},{3,1},{4,6},{5,7},{6,4},{7,5},{8,10},{9,11},{10,... | collective-permute-start | bytes 417800 | tf_op jit(solution)/shard_map/ppermute | solution.py:134
  24.4 2.9 %load_kernel.1 = (bf16[1,2048,512]{2,1,0:T(8,128)(2,1)S(1)}, bf16[1,2048,512]{2,1,0:T(8,128)(2,1)S(1)}, bf16[1,512,2048]{2,1,0:T(8,128)(2,1)S(1)}) custom-call(bf16[1,2048,512]{2,1,0:T(8,128)(2,1)} %refs_0_.1, bf16[1,2048,512]{2,1,0:T(8,128)(2,1)} %refs_1_.3, bf16[1,512,2048]{2,1,0:T(8,128)(2,1)} %refs_2_.1), custom_call_target="tpu_custom_call" | custom-call | tf_op jit(solution)/shard_map/load_kernel/pallas_call | solution.py:159
  27.3 0.0 collective-permute-done.3.refs_8_.refs_6_
  27.3 0.0 collective-permute-done.4.refs_9_.refs_7_
  27.3 0.0 collective-permute-done.5.refs_10_.refs_8_
  27.4 4.3 %expert_kernel.3 = (f32[32,2048]{1,0:T(8,128)S(1)}, f32[32,2048]{1,0:T(8,128)S(1)}, bf16[32,2048]{1,0:T(8,128)(2,1)S(1)}, bf16[32,2048]{1,0:T(8,128)(2,1)S(1)}) custom-call(s32[1,128]{1,0:T(1,128)S(1)} %get-tuple-element.18.refs_0_, bf16[32,2176]{1,0:T(8,128)(2,1)S(1)} %get-tuple-element.19.refs_1_, bf16[32,2176]{1,0:T(8,128)(2,1)S(1)} %collective-permute-done.refs_2_, ...), custom_call_target="tpu_custom_call" | custom-call | tf_op jit(solution)/shard_map/expert_kernel/pallas_call | solution.py:175
  31.6 1.5 %collective-permute-start.7 = (bf16[32,2048]{1,0:T(8,128)(2,1)S(1)}, bf16[32,2048]{1,0:T(8,128)(2,1)S(1)}, u32[]{:S(2)}, u32[]{:S(2)}) collective-permute-start(bf16[32,2048]{1,0:T(8,128)(2,1)S(1)} %get-tuple-element.26), channel_id=1, source_target_pairs={{0,2},{1,3},{2,0},{3,1},{4,6},{5,7},{6,4},{7,5},{8,10},{9,11},{10,... | collective-permute-start | bytes 393224 | tf_op jit(solution)/shard_map/ppermute | solution.py:134
  33.1 0.6 %collective-permute-start.6 = (bf16[32,2048]{1,0:T(8,128)(2,1)S(1)}, bf16[32,2048]{1,0:T(8,128)(2,1)S(1)}, u32[]{:S(2)}, u32[]{:S(2)}) collective-permute-start(bf16[32,2048]{1,0:T(8,128)(2,1)S(1)} %get-tuple-element.24), channel_id=1, source_target_pairs={{0,2},{1,3},{2,0},{3,1},{4,6},{5,7},{6,4},{7,5},{8,10},{9,11},{10,... | collective-permute-start | bytes 393224 | tf_op jit(solution)/shard_map/ppermute | solution.py:134
  33.7 0.0 collective-permute-done.14.refs_2_
  33.7 4.7 %expert_kernel.5 = (f32[32,2048]{1,0:T(8,128)S(1)}, bf16[32,2048]{1,0:T(8,128)(2,1)S(1)}) custom-call(s32[1,128]{1,0:T(1,128)S(1)} %get-tuple-element.18.refs_0_, bf16[32,2176]{1,0:T(8,128)(2,1)S(1)} %collective-permute-done.13.refs_1_, bf16[32,2176]{1,0:T(8,128)(2,1)S(1)} %collective-permute-done.14.refs_2_, ...), custom_call_target="tpu_custom_call" | custom-call | tf_op jit(solution)/shard_map/expert_kernel/pallas_call | solution.py:175
  38.4 1.5 %collective-permute-start.15 = (bf16[32,2048]{1,0:T(8,128)(2,1)S(1)}, bf16[32,2048]{1,0:T(8,128)(2,1)S(1)}, u32[]{:S(2)}, u32[]{:S(2)}) collective-permute-start(bf16[32,2048]{1,0:T(8,128)(2,1)S(1)} %get-tuple-element.30), channel_id=1, source_target_pairs={{0,2},{1,3},{2,0},{3,1},{4,6},{5,7},{6,4},{7,5},{8,10},{9,11},{10,... | collective-permute-start | bytes 393224 | tf_op jit(solution)/shard_map/ppermute | solution.py:134
  39.9 0.0 collective-permute-done.10.refs_2_
  39.9 4.7 %expert_kernel.4 = (f32[32,2048]{1,0:T(8,128)S(1)}, bf16[32,2048]{1,0:T(8,128)(2,1)S(1)}) custom-call(s32[1,128]{1,0:T(1,128)S(1)} %get-tuple-element.18.refs_0_, bf16[32,2176]{1,0:T(8,128)(2,1)S(1)} %collective-permute-done.9.refs_1_, bf16[32,2176]{1,0:T(8,128)(2,1)S(1)} %collective-permute-done.10.refs_2_, ...), custom_call_target="tpu_custom_call" | custom-call | tf_op jit(solution)/shard_map/expert_kernel/pallas_call | solution.py:175
  44.5 0.0 copy-start
  44.5 0.7 %collective-permute-start.11 = (bf16[32,2048]{1,0:T(8,128)(2,1)S(1)}, bf16[32,2048]{1,0:T(8,128)(2,1)S(1)}, u32[]{:S(2)}, u32[]{:S(2)}) collective-permute-start(bf16[32,2048]{1,0:T(8,128)(2,1)S(1)} %get-tuple-element.28), channel_id=1, source_target_pairs={{0,2},{1,3},{2,0},{3,1},{4,6},{5,7},{6,4},{7,5},{8,10},{9,11},{10,... | collective-permute-start | bytes 393224 | tf_op jit(solution)/shard_map/ppermute | solution.py:134
  45.2 0.0 collective-permute-done.7
  45.3 0.1 collective-permute-start.8
  45.4 0.0 collective-permute-done.15
  45.4 3.5 %collective-permute-start.16 = (bf16[32,2048]{1,0:T(8,128)(2,1)S(1)}, bf16[32,2048]{1,0:T(8,128)(2,1)S(1)}, u32[]{:S(2)}, u32[]{:S(2)}) collective-permute-start(bf16[32,2048]{1,0:T(8,128)(2,1)S(1)} %add_convert_fusion), channel_id=1, source_target_pairs={{0,12},{1,13},{2,14},{3,15},{4,8},{5,9},{6,10},{7,11},{8,4},{9,5},... | collective-permute-start | bytes 393224 | tf_op jit(solution)/shard_map/ppermute | solution.py:134
  48.9 0.7 %collective-permute-done.11 = bf16[32,2048]{1,0:T(8,128)(2,1)S(1)} collective-permute-done((bf16[32,2048]{1,0:T(8,128)(2,1)S(1)}, bf16[32,2048]{1,0:T(8,128)(2,1)S(1)}, u32[]{:S(2)}, u32[]{:S(2)}) %collective-permute-start.11) | collective-permute-done | bytes 131104 | tf_op jit(solution)/shard_map/ppermute | solution.py:134
  49.6 0.1 collective-permute-start.12
  49.7 0.0 collective-permute-done.6
  49.7 1.9 %collective-permute-done.8.refs_1_ = bf16[32,2048]{1,0:T(8,128)(2,1)S(1)} collective-permute-done((bf16[32,2048]{1,0:T(8,128)(2,1)S(1)}, bf16[32,2048]{1,0:T(8,128)(2,1)S(1)}, u32[]{:S(2)}, u32[]{:S(2)}) %collective-permute-start.8) | collective-permute-done | bytes 131104 | tf_op jit(solution)/shard_map/ppermute | solution.py:134
  51.7 1.6 %collective-permute-done.16.refs_3_ = bf16[32,2048]{1,0:T(8,128)(2,1)S(1)} collective-permute-done((bf16[32,2048]{1,0:T(8,128)(2,1)S(1)}, bf16[32,2048]{1,0:T(8,128)(2,1)S(1)}, u32[]{:S(2)}, u32[]{:S(2)}) %collective-permute-start.16) | collective-permute-done | bytes 131104 | tf_op jit(solution)/shard_map/ppermute | solution.py:134
  53.2 3.6 %collective-permute-done.12.refs_2_ = bf16[32,2048]{1,0:T(8,128)(2,1)S(1)} collective-permute-done((bf16[32,2048]{1,0:T(8,128)(2,1)S(1)}, bf16[32,2048]{1,0:T(8,128)(2,1)S(1)}, u32[]{:S(2)}, u32[]{:S(2)}) %collective-permute-start.12) | collective-permute-done | bytes 131104 | tf_op jit(solution)/shard_map/ppermute | solution.py:134
  56.8 0.0 copy-done
  56.8 0.8 %finish_kernel.1 = bf16[32,2048]{1,0:T(8,128)(2,1)} custom-call(f32[32,2048]{1,0:T(8,128)S(1)} %convert_add_fusion.refs_0_, bf16[32,2048]{1,0:T(8,128)(2,1)S(1)} %collective-permute-done.8.refs_1_, bf16[32,2048]{1,0:T(8,128)(2,1)S(1)} %collective-permute-done.12.refs_2_, bf16[32,2048]{1,0:T(8,128)(2,1)S(1)} %collective-permute-done.16.refs_3_, ...), custom_call_target="tpu_custom_call" | custom-call | tf_op jit(solution)/shard_map/finish_kernel/pallas_call | solution.py:186
  (4 shorter events, 0.1 us)
Async XLA Ops:
  0.0 27.3 %collective-permute-start.3 = (bf16[1,2048,512]{2,1,0:T(8,128)(2,1)}, bf16[1,2048,512]{2,1,0:T(8,128)(2,1)S(1)}, u32[]{:S(2)}, u32[]{:S(2)}) collective-permute-start(bf16[1,2048,512]{2,1,0:T(8,128)(2,1)} %refs_0_.1), channel_id=1, source_target_pairs={{0,1},{1,0},{2,3},{3,2},{4,5},{5,4},{6,7},{7,6},{8,9},{9,8},{10,11... | collective-permute-start | bytes 6291464 | tf_op jit(solution)/shard_map/ppermute | solution.py:134
  0.5 26.8 %collective-permute-start.4 = (bf16[1,2048,512]{2,1,0:T(8,128)(2,1)}, bf16[1,2048,512]{2,1,0:T(8,128)(2,1)}, u32[]{:S(2)}, u32[]{:S(2)}) collective-permute-start(bf16[1,2048,512]{2,1,0:T(8,128)(2,1)} %refs_1_.3), channel_id=1, source_target_pairs={{0,1},{1,0},{2,3},{3,2},{4,5},{5,4},{6,7},{7,6},{8,9},{9,8},{10,11... | collective-permute-start | bytes 6291464 | tf_op jit(solution)/shard_map/ppermute | solution.py:134
  0.5 26.8 %collective-permute-start.5 = (bf16[1,512,2048]{2,1,0:T(8,128)(2,1)}, bf16[1,512,2048]{2,1,0:T(8,128)(2,1)}, u32[]{:S(2)}, u32[]{:S(2)}) collective-permute-start(bf16[1,512,2048]{2,1,0:T(8,128)(2,1)} %refs_2_.1), channel_id=1, source_target_pairs={{0,1},{1,0},{2,3},{3,2},{4,5},{5,4},{6,7},{7,6},{8,9},{9,8},{10,11... | collective-permute-start | bytes 6291464 | tf_op jit(solution)/shard_map/ppermute | solution.py:134
  2.1 9.8 %collective-permute-start = (bf16[32,2176]{1,0:T(8,128)(2,1)S(1)}, bf16[32,2176]{1,0:T(8,128)(2,1)S(1)}, u32[]{:S(2)}, u32[]{:S(2)}) collective-permute-start(bf16[32,2176]{1,0:T(8,128)(2,1)S(1)} %get-tuple-element.19.refs_1_), channel_id=1, source_target_pairs={{0,4},{1,5},{2,6},{3,7},{4,0},{5,1},{6,2},{7,3},{8,12},{9,13},{10,... | collective-permute-start | bytes 417800 | tf_op jit(solution)/shard_map/ppermute | solution.py:134
  4.7 9.7 %collective-permute-start.9 = (bf16[32,2176]{1,0:T(8,128)(2,1)S(1)}, bf16[32,2176]{1,0:T(8,128)(2,1)S(1)}, u32[]{:S(2)}, u32[]{:S(2)}) collective-permute-start(bf16[32,2176]{1,0:T(8,128)(2,1)S(1)} %get-tuple-element.19.refs_1_), channel_id=1, source_target_pairs={{0,8},{1,9},{2,10},{3,11},{4,12},{5,13},{6,14},{7,15},{8,0},{9,1},... | collective-permute-start | bytes 417800 | tf_op jit(solution)/shard_map/ppermute | solution.py:134
  11.9 5.3 %collective-permute-start.1 = (bf16[32,2176]{1,0:T(8,128)(2,1)S(1)}, bf16[32,2176]{1,0:T(8,128)(2,1)S(1)}, u32[]{:S(2)}, u32[]{:S(2)}) collective-permute-start(bf16[32,2176]{1,0:T(8,128)(2,1)S(1)} %get-tuple-element.19.refs_1_), channel_id=1, source_target_pairs={{0,2},{1,3},{2,0},{3,1},{4,6},{5,7},{6,4},{7,5},{8,10},{9,11},{10,... | collective-permute-start | bytes 417800 | tf_op jit(solution)/shard_map/ppermute | solution.py:134
  14.5 5.1 %collective-permute-start.13 = (bf16[32,2176]{1,0:T(8,128)(2,1)S(1)}, bf16[32,2176]{1,0:T(8,128)(2,1)S(1)}, u32[]{:S(2)}, u32[]{:S(2)}) collective-permute-start(bf16[32,2176]{1,0:T(8,128)(2,1)S(1)} %collective-permute-done.9.refs_1_), channel_id=1, source_target_pairs={{0,4},{1,5},{2,6},{3,7},{4,0},{5,1},{6,2},{7,3},{8,12},{9,13},{10,... | collective-permute-start | bytes 417800 | tf_op jit(solution)/shard_map/ppermute | solution.py:134
  17.3 6.5 %collective-permute-start.2 = (bf16[32,2176]{1,0:T(8,128)(2,1)S(1)}, bf16[32,2176]{1,0:T(8,128)(2,1)S(1)}, u32[]{:S(2)}, u32[]{:S(2)}) collective-permute-start(bf16[32,2176]{1,0:T(8,128)(2,1)S(1)} %collective-permute-done.refs_2_), channel_id=1, source_target_pairs={{0,2},{1,3},{2,0},{3,1},{4,6},{5,7},{6,4},{7,5},{8,10},{9,11},{10,... | collective-permute-start | bytes 417800 | tf_op jit(solution)/shard_map/ppermute | solution.py:134
  19.5 14.2 %collective-permute-start.14 = (bf16[32,2176]{1,0:T(8,128)(2,1)S(1)}, bf16[32,2176]{1,0:T(8,128)(2,1)S(1)}, u32[]{:S(2)}, u32[]{:S(2)}) collective-permute-start(bf16[32,2176]{1,0:T(8,128)(2,1)S(1)} %collective-permute-done.13.refs_1_), channel_id=1, source_target_pairs={{0,2},{1,3},{2,0},{3,1},{4,6},{5,7},{6,4},{7,5},{8,10},{9,11},{10,... | collective-permute-start | bytes 417800 | tf_op jit(solution)/shard_map/ppermute | solution.py:134
  23.8 16.1 %collective-permute-start.10 = (bf16[32,2176]{1,0:T(8,128)(2,1)S(1)}, bf16[32,2176]{1,0:T(8,128)(2,1)S(1)}, u32[]{:S(2)}, u32[]{:S(2)}) collective-permute-start(bf16[32,2176]{1,0:T(8,128)(2,1)S(1)} %collective-permute-done.9.refs_1_), channel_id=1, source_target_pairs={{0,2},{1,3},{2,0},{3,1},{4,6},{5,7},{6,4},{7,5},{8,10},{9,11},{10,... | collective-permute-start | bytes 417800 | tf_op jit(solution)/shard_map/ppermute | solution.py:134
  31.6 13.6 %collective-permute-start.7 = (bf16[32,2048]{1,0:T(8,128)(2,1)S(1)}, bf16[32,2048]{1,0:T(8,128)(2,1)S(1)}, u32[]{:S(2)}, u32[]{:S(2)}) collective-permute-start(bf16[32,2048]{1,0:T(8,128)(2,1)S(1)} %get-tuple-element.26), channel_id=1, source_target_pairs={{0,2},{1,3},{2,0},{3,1},{4,6},{5,7},{6,4},{7,5},{8,10},{9,11},{10,... | collective-permute-start | bytes 393224 | tf_op jit(solution)/shard_map/ppermute | solution.py:134
  33.1 16.6 %collective-permute-start.6 = (bf16[32,2048]{1,0:T(8,128)(2,1)S(1)}, bf16[32,2048]{1,0:T(8,128)(2,1)S(1)}, u32[]{:S(2)}, u32[]{:S(2)}) collective-permute-start(bf16[32,2048]{1,0:T(8,128)(2,1)S(1)} %get-tuple-element.24), channel_id=1, source_target_pairs={{0,2},{1,3},{2,0},{3,1},{4,6},{5,7},{6,4},{7,5},{8,10},{9,11},{10,... | collective-permute-start | bytes 393224 | tf_op jit(solution)/shard_map/ppermute | solution.py:134
  38.4 7.0 %collective-permute-start.15 = (bf16[32,2048]{1,0:T(8,128)(2,1)S(1)}, bf16[32,2048]{1,0:T(8,128)(2,1)S(1)}, u32[]{:S(2)}, u32[]{:S(2)}) collective-permute-start(bf16[32,2048]{1,0:T(8,128)(2,1)S(1)} %get-tuple-element.30), channel_id=1, source_target_pairs={{0,2},{1,3},{2,0},{3,1},{4,6},{5,7},{6,4},{7,5},{8,10},{9,11},{10,... | collective-permute-start | bytes 393224 | tf_op jit(solution)/shard_map/ppermute | solution.py:134
  44.5 12.3 %copy-start = (f32[2048]{0:T(1024)S(1)}, f32[2048]{0:T(1024)}, u32[]{:S(2)}) copy-start(f32[2048]{0:T(1024)} %param.15) | copy-start | bytes 24580
  44.5 5.0 %collective-permute-start.11 = (bf16[32,2048]{1,0:T(8,128)(2,1)S(1)}, bf16[32,2048]{1,0:T(8,128)(2,1)S(1)}, u32[]{:S(2)}, u32[]{:S(2)}) collective-permute-start(bf16[32,2048]{1,0:T(8,128)(2,1)S(1)} %get-tuple-element.28), channel_id=1, source_target_pairs={{0,2},{1,3},{2,0},{3,1},{4,6},{5,7},{6,4},{7,5},{8,10},{9,11},{10,... | collective-permute-start | bytes 393224 | tf_op jit(solution)/shard_map/ppermute | solution.py:134
  45.3 6.4 %collective-permute-start.8 = (bf16[32,2048]{1,0:T(8,128)(2,1)S(1)}, bf16[32,2048]{1,0:T(8,128)(2,1)S(1)}, u32[]{:S(2)}, u32[]{:S(2)}) collective-permute-start(bf16[32,2048]{1,0:T(8,128)(2,1)S(1)} %add_convert_fusion.2), channel_id=1, source_target_pairs={{0,4},{1,5},{2,6},{3,7},{4,0},{5,1},{6,2},{7,3},{8,12},{9,13},{10,... | collective-permute-start | bytes 393224 | tf_op jit(solution)/shard_map/ppermute | solution.py:134
  45.4 7.8 %collective-permute-start.16 = (bf16[32,2048]{1,0:T(8,128)(2,1)S(1)}, bf16[32,2048]{1,0:T(8,128)(2,1)S(1)}, u32[]{:S(2)}, u32[]{:S(2)}) collective-permute-start(bf16[32,2048]{1,0:T(8,128)(2,1)S(1)} %add_convert_fusion), channel_id=1, source_target_pairs={{0,12},{1,13},{2,14},{3,15},{4,8},{5,9},{6,10},{7,11},{8,4},{9,5},... | collective-permute-start | bytes 393224 | tf_op jit(solution)/shard_map/ppermute | solution.py:134
  49.6 7.2 %collective-permute-start.12 = (bf16[32,2048]{1,0:T(8,128)(2,1)S(1)}, bf16[32,2048]{1,0:T(8,128)(2,1)S(1)}, u32[]{:S(2)}, u32[]{:S(2)}) collective-permute-start(bf16[32,2048]{1,0:T(8,128)(2,1)S(1)} %add_convert_fusion.1), channel_id=1, source_target_pairs={{0,8},{1,9},{2,10},{3,11},{4,12},{5,13},{6,14},{7,15},{8,0},{9,1},... | collective-permute-start | bytes 393224 | tf_op jit(solution)/shard_map/ppermute | solution.py:134

commit v3 on v2

--- a/solution.py
+++ b/solution.py
@@ -9,10 +9,11 @@
 QUAD = 4
 PARTS = 3
 MERGE = 2
+FILL = 128
 
 
 def pack_kernel(
-    me_ref, tokens_hbm, routing_hbm, weights_hbm, gain_hbm, out_ref, place_ref, tokens_ref, routing_ref, weights_ref,
+    tokens_hbm, routing_hbm, weights_hbm, gain_hbm, out_ref, place_ref, tokens_ref, routing_ref, weights_ref,
     gain_ref, sems, *, experts, extra
 ):
     copies = [
@@ -30,7 +31,7 @@
         copy.start()
     for copy in copies:
         copy.wait()
-    place_ref[...] = jnp.full(place_ref.shape, me_ref[0], jnp.int32)
+    place_ref[...] = jnp.full(place_ref.shape, lax.axis_index("ep"), jnp.int32)
     rows, width = tokens_ref.shape
     floats = tokens_ref[...].astype(jnp.float32)
     scale = lax.rsqrt(jnp.mean(floats * floats, axis=-1, keepdims=True) + epsilon)
@@ -71,35 +72,45 @@
         copy.wait()
 
 
-def expert_kernel(*refs, experts, count):
-    place_ref, blocks, rest = refs[0], refs[1 : 1 + 2 * count], refs[1 + 2 * count :]
-    weights, outs = rest[:6], rest[6:]
+def expert_kernel(place_ref, *refs, experts, count):
+    blocks, weights, outs = refs[: 2 * count], refs[2 * count :][:6], refs[2 * count + 6 :]
     rows, width = outs[0].shape
     both = jnp.concatenate([block[...] for block in blocks], axis=0)
+    if both.shape[0] < FILL:
+        both = jnp.concatenate([both] * (FILL // both.shape[0]), axis=0)
     values = both[:, :width]
     table = both[:, width:].astype(jnp.float32)
     lane = lax.broadcasted_iota(jnp.int32, table.shape, 1)
-    total = None
-    for bit, (gate_ref, up_ref, down_ref) in enumerate((weights[:3], weights[3:])):
+    hiddens, shares = [], []
+    for bit in range(2):
+        gate_ref, up_ref, _ = weights[3 * bit : 3 * bit + 3]
         chosen = (lane % experts == (place_ref[:, :1] ^ bit)) & (lane < PARTS * experts)
-        weight = jnp.sum(jnp.where(chosen, table, 0.0), axis=1, keepdims=True)
+        shares.append(jnp.sum(jnp.where(chosen, table, 0.0), axis=1, keepdims=True))
         gate = jnp.dot(values, gate_ref[0], preferred_element_type=jnp.float32)
         upward = jnp.dot(values, up_ref[0], preferred_element_type=jnp.float32)
-        hidden = (gate / (1.0 + jnp.exp(-gate)) * upward).astype(jnp.bfloat16)
-        served = jnp.dot(hidden, down_ref[0], preferred_element_type=jnp.float32) * weight
-        total = served if total is None else total + served
+        hiddens.append((gate / (1.0 + jnp.exp(-gate)) * upward).astype(jnp.bfloat16))
+    first, second = [
+        jnp.dot(hidden, weights[3 * bit + 2][0], preferred_element_type=jnp.float32)
+        for bit, hidden in enumerate(hiddens)
+    ]
+    total = first * shares[0] + second * shares[1]
     for i in range(count):
-        outs[i][...] = total[i * rows : (i + 1) * rows]
-        outs[count + i][...] = total[(count + i) * rows : (count + i + 1) * rows].astype(
-            jnp.bfloat16
-        )
+        own = total[i * rows : (i + 1) * rows]
+        other = total[(count + i) * rows : (count + i + 1) * rows]
+        if i == 0:
+            outs[0][...] = own
+            outs[1][...] = other.astype(outs[1].dtype)
+        else:
+            outs[1 + i][:rows] = own.astype(outs[1 + i].dtype)
+            outs[1 + i][rows:] = other.astype(outs[1 + i].dtype)
 
 
 def finish_kernel(*refs):
     *parts, gain_ref, out_ref = refs
+    rows = out_ref.shape[0]
     mixture = parts[0][...].astype(jnp.float32)
     for part in parts[1:]:
-        mixture = mixture + part[...].astype(jnp.float32)
+        mixture = mixture + part[:rows].astype(jnp.float32)
     scale = lax.rsqrt(jnp.mean(mixture * mixture, axis=-1, keepdims=True) + epsilon)
     out_ref[...] = (mixture * scale * gain_ref[...]).astype(jnp.bfloat16)
 
@@ -110,7 +121,6 @@
 
 IN_HBM = pl.BlockSpec(memory_space=pltpu.HBM)
 IN_VMEM = pl.BlockSpec(memory_space=pltpu.VMEM)
-IN_SMEM = pl.BlockSpec(memory_space=pltpu.SMEM)
 
 
 def low(j):
@@ -128,7 +138,6 @@
     choices = routing.shape[1]
     extra = -(-PARTS * devices // 128) * 128
     slabs = devices // QUAD
-    me = lax.axis_index("ep").astype(jnp.int32).reshape(1)
 
     def swap(values, bits):
         return lax.ppermute(values, "ep", [(i, i ^ bits) for i in range(devices)])
@@ -139,7 +148,7 @@
             jax.ShapeDtypeStruct((rows, width + extra), jnp.bfloat16),
             jax.ShapeDtypeStruct((1, 128), jnp.int32),
         ),
-        in_specs=[IN_SMEM] + [IN_HBM] * 4,
+        in_specs=[IN_HBM] * 4,
         out_specs=(IN_VMEM, IN_VMEM),
         scratch_shapes=[
             pltpu.VMEM((rows, width), tokens.dtype),
@@ -150,11 +159,16 @@
         ],
         name="pack_kernel",
         compiler_params=pltpu.CompilerParams(vmem_limit_bytes=4 << 20),
-    )(me, *map(in_hbm, (tokens, routing.T, gate_weights.T, pre_gain.reshape(1, width))))
-
-    blocks = {0: packed}
+    )(*map(in_hbm, (tokens, routing.T, gate_weights.T, pre_gain.reshape(1, width))))
+
+    blocks, across = {0: packed}, {0: swap(packed, 2)}
     for j in range(1, slabs):
-        blocks[j] = swap(blocks[j ^ low(j)], QUAD * low(j))
+        bits, parent = QUAD * low(j), j ^ low(j)
+        blocks[j] = swap(blocks[parent], bits)
+        if parent:
+            across[j] = swap(across[parent], bits)
+        else:
+            across[j] = swap(blocks[j], 2)
 
     weights = pl.pallas_call(
         load_kernel,
@@ -168,27 +182,35 @@
 
     weights = [*weights] + [swap(w, 1) for w in (w_gate, w_up, w_down)]
 
-    across = {j: swap(blocks[j], 2) for j in range(slabs)}
-    home = {}
-    for members in groups_of(slabs).values():
+    home = []
+    for g, members in groups_of(slabs).items():
         count = len(members)
-        served = pl.pallas_call(
+        own, other, *near = pl.pallas_call(
             lambda *refs: expert_kernel(*refs, experts=devices, count=count),
-            out_shape=[jax.ShapeDtypeStruct((rows, width), jnp.float32)] * count
-            + [jax.ShapeDtypeStruct((rows, width), jnp.bfloat16)] * count,
+            out_shape=[
+                jax.ShapeDtypeStruct((rows, width), jnp.float32),
+                jax.ShapeDtypeStruct((rows, width), jnp.float32 if g == 0 else jnp.bfloat16),
+            ]
+            + [jax.ShapeDtypeStruct((2 * rows, width), jnp.bfloat16)] * (count - 1),
             in_specs=[IN_VMEM] * (7 + 2 * count),
             name="expert_kernel",
             compiler_params=pltpu.CompilerParams(vmem_limit_bytes=20 << 20),
         )(place, *[blocks[j] for j in members], *[across[j] for j in members], *weights)
-        for j, keep, send in zip(members, served[:count], served[count:]):
-            total = keep + swap(send, 2).astype(jnp.float32)
-            home[j] = swap(total.astype(jnp.bfloat16), QUAD * j) if j else total
+        near = [swap(part, QUAD * j) for j, part in zip(members[1:], near)]
+        for part in near:
+            other = other + part[rows:].astype(jnp.float32)
+        back = swap(other.astype(jnp.bfloat16), 2)
+        if g:
+            total = (own + back.astype(jnp.float32)).astype(jnp.bfloat16)
+            home.append(swap(total, QUAD * g))
+        else:
+            home += [own, back, *near]
     return pl.pallas_call(
         finish_kernel,
         out_shape=jax.ShapeDtypeStruct((rows, width), jnp.bfloat16),
         name="finish_kernel",
         compiler_params=pltpu.CompilerParams(vmem_limit_bytes=4 << 20),
-    )(*[home[j] for j in range(slabs)], post_gain.reshape(1, width))
+    )(*home, post_gain.reshape(1, width))
 
 
 def solution(mesh):

time: 57.8 us -> 47.4 us (0.82)
  Pallas kernels: 18.4 us -> 10.4 us
  waiting for transfers between devices: 19.2 us -> 13.3 us
  starting transfers between devices: 19.8 us -> 23.4 us
    pallas_call x3, Pallas kernels: 13.6 us -> 5.6 us  [body(): pl.pallas_call(lambda *refs: expert_kernel(*refs, experts=devices, count=...]
    ppermute x17 -> x16, waiting for transfers between devices: 19.2 us -> 13.3 us  [swap(): return lax.ppermute(values, 'ep', [(i, i ^ bits) for i in range(devices)])]
    ppermute x17 -> x16, starting transfers between devices: 19.8 us -> 23.4 us  [swap(): return lax.ppermute(values, 'ep', [(i, i ^ bits) for i in range(devices)])]
  transfers between devices with their start and end apart: 17 -> 16, of which waited for: 9 -> 4; matrix products, arithmetic and copies ran while one was open for 0% -> 0% of each run, Pallas kernels for 30% -> 20%
where the time goes in v3:
time: 47.4 us; the launch traced here: 47.3 us
  starting transfers between devices  23.4 us (49%)
  waiting for transfers between devices  13.3 us (28%)
  Pallas kernels  10.4 us (22%)
    ppermute x16, starting transfers between devices, swap(): return lax.ppermute(values, 'ep', [(i, i ^ bits) for i in range(devices)])  23.4 us
    ppermute x16, waiting for transfers between devices, swap(): return lax.ppermute(values, 'ep', [(i, i ^ bits) for i in range(devices)])  13.3 us
    pallas_call x3, Pallas kernels, body(): pl.pallas_call(lambda *refs: expert_kernel(*refs, experts=devices, count=...  5.6 us
    pallas_call x1, Pallas kernels, body(): pl.pallas_call(load_kernel, out_shape=[jax.ShapeDtypeStruct(w.shape, w.dt...  2.88 us
    pallas_call x1, Pallas kernels, body(): pl.pallas_call(lambda *refs: pack_kernel(*refs, experts=devices, extra=ex...  1.08 us
  transfers between devices with their start and end apart: 16, of which 4 were waited for; matrix products, arithmetic and copies ran while one was open for 0% of the time, Pallas kernels for 20%

profile of v3, /device:TPU:0, one launch (start us, length us, event | category | flops | bytes accessed | tf_op | source)
XLA Modules:
  0.0 47.3 jit_solution(17297747944659762670)
XLA Ops:
  0.0 0.5 %collective-permute-start.3 = (bf16[1,2048,512]{2,1,0:T(8,128)(2,1)}, bf16[1,2048,512]{2,1,0:T(8,128)(2,1)S(1)}, u32[]{:S(2)}, u32[]{:S(2)}) collective-permute-start(bf16[1,2048,512]{2,1,0:T(8,128)(2,1)} %refs_0_.3), channel_id=1, source_target_pairs={{0,1},{1,0},{2,3},{3,2},{4,5},{5,4},{6,7},{7,6},{8,9},{9,8},{10,11... | collective-permute-start | bytes 6291464 | tf_op jit(solution)/shard_map/ppermute | solution.py:143
  0.5 0.0 collective-permute-start.4
  0.5 0.5 %collective-permute-start.5 = (bf16[1,512,2048]{2,1,0:T(8,128)(2,1)}, bf16[1,512,2048]{2,1,0:T(8,128)(2,1)S(1)}, u32[]{:S(2)}, u32[]{:S(2)}) collective-permute-start(bf16[1,512,2048]{2,1,0:T(8,128)(2,1)} %refs_2_.1), channel_id=1, source_target_pairs={{0,1},{1,0},{2,3},{3,2},{4,5},{5,4},{6,7},{7,6},{8,9},{9,8},{10,11... | collective-permute-start | bytes 6291464 | tf_op jit(solution)/shard_map/ppermute | solution.py:143
  1.0 1.1 %pack_kernel.1 = (bf16[32,2176]{1,0:T(8,128)(2,1)S(1)}, s32[1,128]{1,0:T(1,128)S(1)}) custom-call(bf16[32,2048]{1,0:T(8,128)(2,1)} %refs_0_.2, s32[4,32]{1,0:T(4,128)} %bitcast.6, f32[4,32]{1,0:T(4,128)} %bitcast.7, f32[1,2048]{1,0:T(1,128)} %bitcast.5), custom_call_target="tpu_custom_call" | custom-call | tf_op jit(solution)/shard_map/pack_kernel/pallas_call | solution.py:145
  2.1 3.6 %collective-permute-start.8 = (bf16[32,2176]{1,0:T(8,128)(2,1)S(1)}, bf16[32,2176]{1,0:T(8,128)(2,1)S(1)}, u32[]{:S(2)}, u32[]{:S(2)}) collective-permute-start(bf16[32,2176]{1,0:T(8,128)(2,1)S(1)} %get-tuple-element.18.refs_1_), channel_id=1, source_target_pairs={{0,8},{1,9},{2,10},{3,11},{4,12},{5,13},{6,14},{7,15},{8,0},{9,1},... | collective-permute-start | bytes 417800 | tf_op jit(solution)/shard_map/ppermute | solution.py:143
  5.7 1.6 %collective-permute-start = (bf16[32,2176]{1,0:T(8,128)(2,1)S(1)}, bf16[32,2176]{1,0:T(8,128)(2,1)S(1)}, u32[]{:S(2)}, u32[]{:S(2)}) collective-permute-start(bf16[32,2176]{1,0:T(8,128)(2,1)S(1)} %get-tuple-element.18.refs_1_), channel_id=1, source_target_pairs={{0,4},{1,5},{2,6},{3,7},{4,0},{5,1},{6,2},{7,3},{8,12},{9,13},{10,... | collective-permute-start | bytes 417800 | tf_op jit(solution)/shard_map/ppermute | solution.py:143
  7.3 5.9 %collective-permute-done.8.refs_1_ = bf16[32,2176]{1,0:T(8,128)(2,1)S(1)} collective-permute-done((bf16[32,2176]{1,0:T(8,128)(2,1)S(1)}, bf16[32,2176]{1,0:T(8,128)(2,1)S(1)}, u32[]{:S(2)}, u32[]{:S(2)}) %collective-permute-start.8) | collective-permute-done | bytes 139296 | tf_op jit(solution)/shard_map/ppermute | solution.py:143
  13.2 1.6 %collective-permute-start.9 = (bf16[32,2176]{1,0:T(8,128)(2,1)S(1)}, bf16[32,2176]{1,0:T(8,128)(2,1)S(1)}, u32[]{:S(2)}, u32[]{:S(2)}) collective-permute-start(bf16[32,2176]{1,0:T(8,128)(2,1)S(1)} %collective-permute-done.8.refs_1_), channel_id=1, source_target_pairs={{0,2},{1,3},{2,0},{3,1},{4,6},{5,7},{6,4},{7,5},{8,10},{9,11},{10,... | collective-permute-start | bytes 417800 | tf_op jit(solution)/shard_map/ppermute | solution.py:143
  14.7 0.0 collective-permute-done.refs_2_
  14.7 0.5 collective-permute-start.1
  15.2 4.5 %collective-permute-done.9.refs_2_ = bf16[32,2176]{1,0:T(8,128)(2,1)S(1)} collective-permute-done((bf16[32,2176]{1,0:T(8,128)(2,1)S(1)}, bf16[32,2176]{1,0:T(8,128)(2,1)S(1)}, u32[]{:S(2)}, u32[]{:S(2)}) %collective-permute-start.9) | collective-permute-done | bytes 139296 | tf_op jit(solution)/shard_map/ppermute | solution.py:143
  19.7 1.6 %collective-permute-start.2 = (bf16[32,2176]{1,0:T(8,128)(2,1)S(1)}, bf16[32,2176]{1,0:T(8,128)(2,1)S(1)}, u32[]{:S(2)}, u32[]{:S(2)}) collective-permute-start(bf16[32,2176]{1,0:T(8,128)(2,1)S(1)} %collective-permute-done.refs_2_), channel_id=1, source_target_pairs={{0,2},{1,3},{2,0},{3,1},{4,6},{5,7},{6,4},{7,5},{8,10},{9,11},{10,... | collective-permute-start | bytes 417800 | tf_op jit(solution)/shard_map/ppermute | solution.py:143
  21.3 0.0 collective-permute-done.3.refs_8_.refs_6_
  21.3 0.6 %collective-permute-start.12 = (bf16[32,2176]{1,0:T(8,128)(2,1)S(1)}, bf16[32,2176]{1,0:T(8,128)(2,1)S(1)}, u32[]{:S(2)}, u32[]{:S(2)}) collective-permute-start(bf16[32,2176]{1,0:T(8,128)(2,1)S(1)} %collective-permute-done.8.refs_1_), channel_id=1, source_target_pairs={{0,4},{1,5},{2,6},{3,7},{4,0},{5,1},{6,2},{7,3},{8,12},{9,13},{10,... | collective-permute-start | bytes 417800 | tf_op jit(solution)/shard_map/ppermute | solution.py:143
  21.9 0.0 collective-permute-done.4.refs_9_.refs_7_
  21.9 1.4 %collective-permute-start.13 = (bf16[32,2176]{1,0:T(8,128)(2,1)S(1)}, bf16[32,2176]{1,0:T(8,128)(2,1)S(1)}, u32[]{:S(2)}, u32[]{:S(2)}) collective-permute-start(bf16[32,2176]{1,0:T(8,128)(2,1)S(1)} %collective-permute-done.9.refs_2_), channel_id=1, source_target_pairs={{0,4},{1,5},{2,6},{3,7},{4,0},{5,1},{6,2},{7,3},{8,12},{9,13},{10,... | collective-permute-start | bytes 417800 | tf_op jit(solution)/shard_map/ppermute | solution.py:143
  23.3 2.9 %load_kernel.1 = (bf16[1,2048,512]{2,1,0:T(8,128)(2,1)S(1)}, bf16[1,2048,512]{2,1,0:T(8,128)(2,1)S(1)}, bf16[1,512,2048]{2,1,0:T(8,128)(2,1)S(1)}) custom-call(bf16[1,2048,512]{2,1,0:T(8,128)(2,1)} %refs_0_.3, bf16[1,2048,512]{2,1,0:T(8,128)(2,1)} %refs_1_.1, bf16[1,512,2048]{2,1,0:T(8,128)(2,1)} %refs_2_.1), custom_call_target="tpu_custom_call" | custom-call | tf_op jit(solution)/shard_map/load_kernel/pallas_call | solution.py:173
  26.2 0.0 collective-permute-done.5.refs_10_.refs_8_
  26.2 1.9 %expert_kernel.4 = (f32[32,2048]{1,0:T(8,128)S(1)}, bf16[32,2048]{1,0:T(8,128)(2,1)S(1)}) custom-call(s32[1,128]{1,0:T(1,128)S(1)} %get-tuple-element.17.refs_0_, bf16[32,2176]{1,0:T(8,128)(2,1)S(1)} %collective-permute-done.8.refs_1_, bf16[32,2176]{1,0:T(8,128)(2,1)S(1)} %collective-permute-done.9.refs_2_, ...), custom_call_target="tpu_custom_call" | custom-call | tf_op jit(solution)/shard_map/expert_kernel/pallas_call | solution.py:188
  28.1 0.5 %collective-permute-start.10 = (bf16[32,2048]{1,0:T(8,128)(2,1)S(1)}, bf16[32,2048]{1,0:T(8,128)(2,1)S(1)}, u32[]{:S(2)}, u32[]{:S(2)}) collective-permute-start(bf16[32,2048]{1,0:T(8,128)(2,1)S(1)} %get-tuple-element.26), channel_id=1, source_target_pairs={{0,2},{1,3},{2,0},{3,1},{4,6},{5,7},{6,4},{7,5},{8,10},{9,11},{10,... | collective-permute-start | bytes 393224 | tf_op jit(solution)/shard_map/ppermute | solution.py:143
  28.6 0.0 collective-permute-done.1.refs_3_
  28.6 0.0 collective-permute-done.2.refs_4_
  28.6 1.9 %expert_kernel.3 = (f32[32,2048]{1,0:T(8,128)S(1)}, f32[32,2048]{1,0:T(8,128)S(1)}, bf16[64,2048]{1,0:T(8,128)(2,1)S(1)}) custom-call(s32[1,128]{1,0:T(1,128)S(1)} %get-tuple-element.17.refs_0_, bf16[32,2176]{1,0:T(8,128)(2,1)S(1)} %get-tuple-element.18.refs_1_, bf16[32,2176]{1,0:T(8,128)(2,1)S(1)} %collective-permute-done.refs_2_, ...), custom_call_target="tpu_custom_call" | custom-call | tf_op jit(solution)/shard_map/expert_kernel/pallas_call | solution.py:188
  30.5 0.0 copy-start
  30.5 0.7 %collective-permute-start.6 = (bf16[64,2048]{1,0:T(8,128)(2,1)S(1)}, bf16[64,2048]{1,0:T(8,128)(2,1)S(1)}, u32[]{:S(2)}, u32[]{:S(2)}) collective-permute-start(bf16[64,2048]{1,0:T(8,128)(2,1)S(1)} %get-tuple-element.24), channel_id=1, source_target_pairs={{0,4},{1,5},{2,6},{3,7},{4,0},{5,1},{6,2},{7,3},{8,12},{9,13},{10,... | collective-permute-start | bytes 786440 | tf_op jit(solution)/shard_map/ppermute | solution.py:143
  31.2 0.0 collective-permute-done.12.refs_1_
  31.2 0.0 collective-permute-done.13.refs_2_
  31.2 1.9 %expert_kernel.5 = (f32[32,2048]{1,0:T(8,128)S(1)}, bf16[32,2048]{1,0:T(8,128)(2,1)S(1)}) custom-call(s32[1,128]{1,0:T(1,128)S(1)} %get-tuple-element.17.refs_0_, bf16[32,2176]{1,0:T(8,128)(2,1)S(1)} %collective-permute-done.12.refs_1_, bf16[32,2176]{1,0:T(8,128)(2,1)S(1)} %collective-permute-done.13.refs_2_, ...), custom_call_target="tpu_custom_call" | custom-call | tf_op jit(solution)/shard_map/expert_kernel/pallas_call | solution.py:188
  33.1 1.6 %collective-permute-start.14 = (bf16[32,2048]{1,0:T(8,128)(2,1)S(1)}, bf16[32,2048]{1,0:T(8,128)(2,1)S(1)}, u32[]{:S(2)}, u32[]{:S(2)}) collective-permute-start(bf16[32,2048]{1,0:T(8,128)(2,1)S(1)} %get-tuple-element.28), channel_id=1, source_target_pairs={{0,2},{1,3},{2,0},{3,1},{4,6},{5,7},{6,4},{7,5},{8,10},{9,11},{10,... | collective-permute-start | bytes 393224 | tf_op jit(solution)/shard_map/ppermute | solution.py:143
  34.7 0.0 collective-permute-done.10
  34.7 3.4 %collective-permute-start.11 = (bf16[32,2048]{1,0:T(8,128)(2,1)S(1)}, bf16[32,2048]{1,0:T(8,128)(2,1)S(1)}, u32[]{:S(2)}, u32[]{:S(2)}) collective-permute-start(bf16[32,2048]{1,0:T(8,128)(2,1)S(1)} %add_convert_fusion.1), channel_id=1, source_target_pairs={{0,8},{1,9},{2,10},{3,11},{4,12},{5,13},{6,14},{7,15},{8,0},{9,1},... | collective-permute-start | bytes 393224 | tf_op jit(solution)/shard_map/ppermute | solution.py:143
  38.1 0.0 collective-permute-done.14
  38.2 2.9 %collective-permute-start.15 = (bf16[32,2048]{1,0:T(8,128)(2,1)S(1)}, bf16[32,2048]{1,0:T(8,128)(2,1)S(1)}, u32[]{:S(2)}, u32[]{:S(2)}) collective-permute-start(bf16[32,2048]{1,0:T(8,128)(2,1)S(1)} %add_convert_fusion), channel_id=1, source_target_pairs={{0,12},{1,13},{2,14},{3,15},{4,8},{5,9},{6,10},{7,11},{8,4},{9,5},... | collective-permute-start | bytes 393224 | tf_op jit(solution)/shard_map/ppermute | solution.py:143
  41.1 0.0 collective-permute-done.6.refs_2_
  41.1 2.4 %collective-permute-start.7 = (bf16[32,2048]{1,0:T(8,128)(2,1)S(1)}, bf16[32,2048]{1,0:T(8,128)(2,1)S(1)}, u32[]{:S(2)}, u32[]{:S(2)}) collective-permute-start(bf16[32,2048]{1,0:T(8,128)(2,1)S(1)} %add_convert_fusion.2), channel_id=1, source_target_pairs={{0,2},{1,3},{2,0},{3,1},{4,6},{5,7},{6,4},{7,5},{8,10},{9,11},{10,... | collective-permute-start | bytes 393224 | tf_op jit(solution)/shard_map/ppermute | solution.py:143
  43.5 2.0 %collective-permute-done.11.refs_3_ = bf16[32,2048]{1,0:T(8,128)(2,1)S(1)} collective-permute-done((bf16[32,2048]{1,0:T(8,128)(2,1)S(1)}, bf16[32,2048]{1,0:T(8,128)(2,1)S(1)}, u32[]{:S(2)}, u32[]{:S(2)}) %collective-permute-start.11) | collective-permute-done | bytes 131104 | tf_op jit(solution)/shard_map/ppermute | solution.py:143
  45.5 0.0 collective-permute-done.15.refs_4_
  45.5 0.9 %collective-permute-done.7.refs_1_ = bf16[32,2048]{1,0:T(8,128)(2,1)S(1)} collective-permute-done((bf16[32,2048]{1,0:T(8,128)(2,1)S(1)}, bf16[32,2048]{1,0:T(8,128)(2,1)S(1)}, u32[]{:S(2)}, u32[]{:S(2)}) %collective-permute-start.7) | collective-permute-done | bytes 131104 | tf_op jit(solution)/shard_map/ppermute | solution.py:143
  46.4 0.0 copy-done
  46.5 0.8 %finish_kernel.1 = bf16[32,2048]{1,0:T(8,128)(2,1)} custom-call(f32[32,2048]{1,0:T(8,128)S(1)} %get-tuple-element.22.refs_0_, bf16[32,2048]{1,0:T(8,128)(2,1)S(1)} %collective-permute-done.7.refs_1_, bf16[64,2048]{1,0:T(8,128)(2,1)S(1)} %collective-permute-done.6.refs_2_, bf16[32,2048]{1,0:T(8,128)(2,1)S(1)} %collective-permute-done.11.refs_3_, ...), custom_call_target="tpu_custom_call" | custom-call | tf_op jit(solution)/shard_map/finish_kernel/pallas_call | solution.py:208
  (3 shorter events, 0.1 us)
Async XLA Ops:
  0.0 21.3 %collective-permute-start.3 = (bf16[1,2048,512]{2,1,0:T(8,128)(2,1)}, bf16[1,2048,512]{2,1,0:T(8,128)(2,1)S(1)}, u32[]{:S(2)}, u32[]{:S(2)}) collective-permute-start(bf16[1,2048,512]{2,1,0:T(8,128)(2,1)} %refs_0_.3), channel_id=1, source_target_pairs={{0,1},{1,0},{2,3},{3,2},{4,5},{5,4},{6,7},{7,6},{8,9},{9,8},{10,11... | collective-permute-start | bytes 6291464 | tf_op jit(solution)/shard_map/ppermute | solution.py:143
  0.5 21.4 %collective-permute-start.4 = (bf16[1,2048,512]{2,1,0:T(8,128)(2,1)}, bf16[1,2048,512]{2,1,0:T(8,128)(2,1)S(1)}, u32[]{:S(2)}, u32[]{:S(2)}) collective-permute-start(bf16[1,2048,512]{2,1,0:T(8,128)(2,1)} %refs_1_.1), channel_id=1, source_target_pairs={{0,1},{1,0},{2,3},{3,2},{4,5},{5,4},{6,7},{7,6},{8,9},{9,8},{10,11... | collective-permute-start | bytes 6291464 | tf_op jit(solution)/shard_map/ppermute | solution.py:143
  0.5 25.7 %collective-permute-start.5 = (bf16[1,512,2048]{2,1,0:T(8,128)(2,1)}, bf16[1,512,2048]{2,1,0:T(8,128)(2,1)S(1)}, u32[]{:S(2)}, u32[]{:S(2)}) collective-permute-start(bf16[1,512,2048]{2,1,0:T(8,128)(2,1)} %refs_2_.1), channel_id=1, source_target_pairs={{0,1},{1,0},{2,3},{3,2},{4,5},{5,4},{6,7},{7,6},{8,9},{9,8},{10,11... | collective-permute-start | bytes 6291464 | tf_op jit(solution)/shard_map/ppermute | solution.py:143
  2.1 11.1 %collective-permute-start.8 = (bf16[32,2176]{1,0:T(8,128)(2,1)S(1)}, bf16[32,2176]{1,0:T(8,128)(2,1)S(1)}, u32[]{:S(2)}, u32[]{:S(2)}) collective-permute-start(bf16[32,2176]{1,0:T(8,128)(2,1)S(1)} %get-tuple-element.18.refs_1_), channel_id=1, source_target_pairs={{0,8},{1,9},{2,10},{3,11},{4,12},{5,13},{6,14},{7,15},{8,0},{9,1},... | collective-permute-start | bytes 417800 | tf_op jit(solution)/shard_map/ppermute | solution.py:143
  5.7 9.0 %collective-permute-start = (bf16[32,2176]{1,0:T(8,128)(2,1)S(1)}, bf16[32,2176]{1,0:T(8,128)(2,1)S(1)}, u32[]{:S(2)}, u32[]{:S(2)}) collective-permute-start(bf16[32,2176]{1,0:T(8,128)(2,1)S(1)} %get-tuple-element.18.refs_1_), channel_id=1, source_target_pairs={{0,4},{1,5},{2,6},{3,7},{4,0},{5,1},{6,2},{7,3},{8,12},{9,13},{10,... | collective-permute-start | bytes 417800 | tf_op jit(solution)/shard_map/ppermute | solution.py:143
  13.2 6.5 %collective-permute-start.9 = (bf16[32,2176]{1,0:T(8,128)(2,1)S(1)}, bf16[32,2176]{1,0:T(8,128)(2,1)S(1)}, u32[]{:S(2)}, u32[]{:S(2)}) collective-permute-start(bf16[32,2176]{1,0:T(8,128)(2,1)S(1)} %collective-permute-done.8.refs_1_), channel_id=1, source_target_pairs={{0,2},{1,3},{2,0},{3,1},{4,6},{5,7},{6,4},{7,5},{8,10},{9,11},{10,... | collective-permute-start | bytes 417800 | tf_op jit(solution)/shard_map/ppermute | solution.py:143
  14.7 13.9 %collective-permute-start.1 = (bf16[32,2176]{1,0:T(8,128)(2,1)S(1)}, bf16[32,2176]{1,0:T(8,128)(2,1)S(1)}, u32[]{:S(2)}, u32[]{:S(2)}) collective-permute-start(bf16[32,2176]{1,0:T(8,128)(2,1)S(1)} %get-tuple-element.18.refs_1_), channel_id=1, source_target_pairs={{0,2},{1,3},{2,0},{3,1},{4,6},{5,7},{6,4},{7,5},{8,10},{9,11},{10,... | collective-permute-start | bytes 417800 | tf_op jit(solution)/shard_map/ppermute | solution.py:143
  19.7 8.9 %collective-permute-start.2 = (bf16[32,2176]{1,0:T(8,128)(2,1)S(1)}, bf16[32,2176]{1,0:T(8,128)(2,1)S(1)}, u32[]{:S(2)}, u32[]{:S(2)}) collective-permute-start(bf16[32,2176]{1,0:T(8,128)(2,1)S(1)} %collective-permute-done.refs_2_), channel_id=1, source_target_pairs={{0,2},{1,3},{2,0},{3,1},{4,6},{5,7},{6,4},{7,5},{8,10},{9,11},{10,... | collective-permute-start | bytes 417800 | tf_op jit(solution)/shard_map/ppermute | solution.py:143
  21.3 10.0 %collective-permute-start.12 = (bf16[32,2176]{1,0:T(8,128)(2,1)S(1)}, bf16[32,2176]{1,0:T(8,128)(2,1)S(1)}, u32[]{:S(2)}, u32[]{:S(2)}) collective-permute-start(bf16[32,2176]{1,0:T(8,128)(2,1)S(1)} %collective-permute-done.8.refs_1_), channel_id=1, source_target_pairs={{0,4},{1,5},{2,6},{3,7},{4,0},{5,1},{6,2},{7,3},{8,12},{9,13},{10,... | collective-permute-start | bytes 417800 | tf_op jit(solution)/shard_map/ppermute | solution.py:143
  21.9 9.3 %collective-permute-start.13 = (bf16[32,2176]{1,0:T(8,128)(2,1)S(1)}, bf16[32,2176]{1,0:T(8,128)(2,1)S(1)}, u32[]{:S(2)}, u32[]{:S(2)}) collective-permute-start(bf16[32,2176]{1,0:T(8,128)(2,1)S(1)} %collective-permute-done.9.refs_2_), channel_id=1, source_target_pairs={{0,4},{1,5},{2,6},{3,7},{4,0},{5,1},{6,2},{7,3},{8,12},{9,13},{10,... | collective-permute-start | bytes 417800 | tf_op jit(solution)/shard_map/ppermute | solution.py:143
  28.1 6.6 %collective-permute-start.10 = (bf16[32,2048]{1,0:T(8,128)(2,1)S(1)}, bf16[32,2048]{1,0:T(8,128)(2,1)S(1)}, u32[]{:S(2)}, u32[]{:S(2)}) collective-permute-start(bf16[32,2048]{1,0:T(8,128)(2,1)S(1)} %get-tuple-element.26), channel_id=1, source_target_pairs={{0,2},{1,3},{2,0},{3,1},{4,6},{5,7},{6,4},{7,5},{8,10},{9,11},{10,... | collective-permute-start | bytes 393224 | tf_op jit(solution)/shard_map/ppermute | solution.py:143
  30.5 15.9 %copy-start = (f32[2048]{0:T(1024)S(1)}, f32[2048]{0:T(1024)}, u32[]{:S(2)}) copy-start(f32[2048]{0:T(1024)} %param.15) | copy-start | bytes 24580
  30.5 10.6 %collective-permute-start.6 = (bf16[64,2048]{1,0:T(8,128)(2,1)S(1)}, bf16[64,2048]{1,0:T(8,128)(2,1)S(1)}, u32[]{:S(2)}, u32[]{:S(2)}) collective-permute-start(bf16[64,2048]{1,0:T(8,128)(2,1)S(1)} %get-tuple-element.24), channel_id=1, source_target_pairs={{0,4},{1,5},{2,6},{3,7},{4,0},{5,1},{6,2},{7,3},{8,12},{9,13},{10,... | collective-permute-start | bytes 786440 | tf_op jit(solution)/shard_map/ppermute | solution.py:143
  33.1 5.0 %collective-permute-start.14 = (bf16[32,2048]{1,0:T(8,128)(2,1)S(1)}, bf16[32,2048]{1,0:T(8,128)(2,1)S(1)}, u32[]{:S(2)}, u32[]{:S(2)}) collective-permute-start(bf16[32,2048]{1,0:T(8,128)(2,1)S(1)} %get-tuple-element.28), channel_id=1, source_target_pairs={{0,2},{1,3},{2,0},{3,1},{4,6},{5,7},{6,4},{7,5},{8,10},{9,11},{10,... | collective-permute-start | bytes 393224 | tf_op jit(solution)/shard_map/ppermute | solution.py:143
  34.7 10.8 %collective-permute-start.11 = (bf16[32,2048]{1,0:T(8,128)(2,1)S(1)}, bf16[32,2048]{1,0:T(8,128)(2,1)S(1)}, u32[]{:S(2)}, u32[]{:S(2)}) collective-permute-start(bf16[32,2048]{1,0:T(8,128)(2,1)S(1)} %add_convert_fusion.1), channel_id=1, source_target_pairs={{0,8},{1,9},{2,10},{3,11},{4,12},{5,13},{6,14},{7,15},{8,0},{9,1},... | collective-permute-start | bytes 393224 | tf_op jit(solution)/shard_map/ppermute | solution.py:143
  38.2 7.4 %collective-permute-start.15 = (bf16[32,2048]{1,0:T(8,128)(2,1)S(1)}, bf16[32,2048]{1,0:T(8,128)(2,1)S(1)}, u32[]{:S(2)}, u32[]{:S(2)}) collective-permute-start(bf16[32,2048]{1,0:T(8,128)(2,1)S(1)} %add_convert_fusion), channel_id=1, source_target_pairs={{0,12},{1,13},{2,14},{3,15},{4,8},{5,9},{6,10},{7,11},{8,4},{9,5},... | collective-permute-start | bytes 393224 | tf_op jit(solution)/shard_map/ppermute | solution.py:143
  41.1 5.3 %collective-permute-start.7 = (bf16[32,2048]{1,0:T(8,128)(2,1)S(1)}, bf16[32,2048]{1,0:T(8,128)(2,1)S(1)}, u32[]{:S(2)}, u32[]{:S(2)}) collective-permute-start(bf16[32,2048]{1,0:T(8,128)(2,1)S(1)} %add_convert_fusion.2), channel_id=1, source_target_pairs={{0,2},{1,3},{2,0},{3,1},{4,6},{5,7},{6,4},{7,5},{8,10},{9,11},{10,... | collective-permute-start | bytes 393224 | tf_op jit(solution)/shard_map/ppermute | solution.py:143
